TPU v7x, 256 devices: a whole 4x4x8 slice. The times are simulated.
256 devices in a mesh: kv: 64 (over z, y, core), tp: 4 (over x).
Axes of the slice: x: 4, y: 4, z: 8, core: 2. Of those that a mesh axis runs over, the one named last changes fastest.
Arguments:
- inputs: bfloat16 [2048, 4096], P(None, 'kv'), may hold values from -150 to 150
- norm_gain: bfloat16 [4096], P('kv'), may hold values from 0.099609375 to 1.8984375
- w_query: bfloat16 [4096, 2048], P('kv', 'tp'), may hold values from -0.09375 to 0.09375
- w_forget: bfloat16 [4096, 2048], P('kv', 'tp'), may hold values from -0.09375 to 0.09375
- w_value: bfloat16 [4096, 2048], P('kv', 'tp'), may hold values from -0.09375 to 0.09375
- lower_bound: float32 [2048], P('tp'), may hold values from 0.05 to 0.9
- head_gain: float32 [2048], P('tp'), may hold values from 0.1 to 1.9
- w_out: bfloat16 [2048, 4096], P('tp', 'kv'), may hold values from -0.125 to 0.125
- prior_state: float32 [512, 16, 128, 128], P('kv', 'tp'), may hold values from -3 to 3
- prev_forget: float32 [512, 4, 2048], P('kv', None, 'tp'), may hold values from 0.3 to 0.97
- prev_values: bfloat16 [512, 4, 2048], P('kv', None, 'tp'), may hold values from -6 to 6
- accepted: int32 [512], P('kv'), may hold values from 0 to 4
Outputs:
- mixed_out: bfloat16 [2048, 4096], P(None, ('kv', 'tp'))
- base_state: float32 [512, 16, 128, 128], P('kv', 'tp')
All inputs are finite; a program needn't handle non-finite values.
Results may differ from a plain program's by a relative error of at most 0.01.
Values may be sent and summed in bfloat16 or wider, within the bound.
A program may use at most 64 MiB of HBM per device.

v0:
```python
import jax
import jax.numpy as jnp
from jax import lax
from jax.sharding import Mesh
from jax.sharding import PartitionSpec as P

D = 4096
KV = ("kv_0", "kv_1", "kv_2")
KV_TP = ("kv_0", "kv_1", "kv_2", "tp")


EPSILON = 1e-06


def side_by_side(arrays, axis, dim, along):
    columns = [a.reshape(*a.shape[:along], -1) for a in arrays]
    both = jnp.concatenate(columns, axis=along)
    out, at, outs = (lax.all_gather(both, axis, axis=dim, tiled=True), 0, [])
    for a, column in zip(arrays, columns):
        section = out[..., at : at + column.shape[along]]
        outs.append(section.reshape(*section.shape[:along], *a.shape[along:]))
        at += column.shape[along]
    return tuple(outs)


def laid_out(blocks, dim):
    lengths = list(blocks.shape[1:])
    lengths[dim] *= blocks.shape[0]
    return jnp.moveaxis(blocks, 0, dim).reshape(lengths)


def gather_in_order(array, axes, sequence):
    blocks = array
    for k in sequence:
        blocks = lax.all_gather(blocks, axes[k])
    done = sequence[::-1]
    back = [done.index(k) for k in range(len(axes))]
    blocks = blocks.transpose(*back, *range(len(axes), blocks.ndim))
    return blocks.reshape(-1, *array.shape)


def gathered_by_axis(array, axes, sequence, dim):
    return laid_out(gather_in_order(array, axes, sequence), dim)


def cut_along(array, dim, size):
    lengths = array.shape
    blocks = array.reshape(*lengths[:dim], size, lengths[dim] // size, *lengths[dim + 1 :])
    return jnp.moveaxis(blocks, dim, 0)


def sum_at_owner(array, axis, dim):
    size = lax.axis_size(axis)
    blocks = lax.all_to_all(cut_along(array, dim, size), axis, 0, 0, tiled=True)
    return jnp.sum(blocks.astype(jnp.float32), axis=0)


def recurrence(
    query_pre,
    forget_pre,
    value_pre,
    lower_bound,
    head_gain,
    prior_state,
    prev_forget,
    prev_values,
    accepted,
):
    sequences = prior_state.shape[0]
    heads = prior_state.shape[1]
    head_size = prior_state.shape[2]
    proposals = prev_forget.shape[1]
    layout = (sequences, proposals, heads, head_size)
    floor_gate = lower_bound.reshape(heads, head_size)
    forget_gate = floor_gate + (1.0 - floor_gate) * jax.nn.sigmoid(forget_pre.reshape(layout))
    keys_new = 1.0 - forget_gate
    queries = jax.nn.silu(query_pre.reshape(layout))
    values = value_pre.reshape(layout)
    old_gate = prev_forget.reshape(layout)
    old_values = prev_values.astype(jnp.float32).reshape(layout)
    carried = prior_state
    for position in range(proposals):
        folded = (
            old_gate[:, position, :, :, None] * carried
            + (1.0 - old_gate[:, position])[..., None] * old_values[:, position, :, None, :]
        )
        taken_up = (position < accepted)[:, None, None, None]
        carried = jnp.where(taken_up, folded, carried)
    base_state = carried
    results = []
    for position in range(proposals):
        carried = (
            forget_gate[:, position, :, :, None] * carried
            + keys_new[:, position, :, :, None] * values[:, position, :, None, :]
        )
        results.append(jnp.einsum("shk,shkv->shv", queries[:, position], carried))
    stacked = jnp.stack(results, axis=1)
    inverse_rms = lax.rsqrt(jnp.mean(stacked * stacked, axis=-1, keepdims=True) + EPSILON)
    normed = stacked * inverse_rms * head_gain.reshape(heads, head_size)
    return (
        normed.astype(jnp.bfloat16).reshape(sequences * proposals, heads * head_size),
        base_state,
    )


def body(
    inputs,
    norm_gain,
    w_query,
    w_forget,
    w_value,
    lower_bound,
    head_gain,
    w_out,
    prior_state,
    prev_forget,
    prev_values,
    accepted,
):
    head_cols = w_query.shape[1]
    stacked_weight = jnp.concatenate((w_query, w_forget, w_value), axis=1)
    own_inputs = lax.all_to_all(inputs, KV, split_axis=0, concat_axis=1, tiled=True)
    widened = own_inputs.astype(jnp.float32)
    squares = jnp.sum(widened * widened, axis=1)
    weight_piece, gain_piece = side_by_side((stacked_weight, norm_gain), KV, 0, 1)
    scaled = (widened * gain_piece.astype(jnp.float32)).astype(jnp.bfloat16)
    projected = jnp.dot(scaled, weight_piece, preferred_element_type=jnp.float32)
    rscale = lax.rsqrt(squares / D + EPSILON)[:, None]
    query_pre = projected[:, :head_cols] * rscale
    forget_pre = projected[:, head_cols : 2 * head_cols] * rscale
    value_pre = projected[:, 2 * head_cols :] * rscale
    normed, base_state = recurrence(
        query_pre,
        forget_pre,
        value_pre,
        lower_bound,
        head_gain,
        prior_state,
        prev_forget,
        prev_values,
        accepted,
    )
    partial_value = jnp.dot(
        gathered_by_axis(normed, KV, (1, 0, 2), 0), w_out, preferred_element_type=jnp.float32
    )
    mixed_out = sum_at_owner(partial_value.astype(jnp.bfloat16), "tp", 1).astype(jnp.bfloat16)
    return (mixed_out, base_state)


def solution(mesh):
    split = Mesh(mesh.devices.reshape(8, 4, 2, mesh.shape["tp"]), ("kv_0", "kv_1", "kv_2", "tp"))
    placed = (
        P(None, KV),
        P(KV),
        P(KV, "tp"),
        P(KV, "tp"),
        P(KV, "tp"),
        P("tp"),
        P("tp"),
        P("tp", KV),
        P(KV, "tp", None, None),
        P(KV, None, "tp"),
        P(KV, None, "tp"),
        P(KV),
    )
    return jax.shard_map(
        body,
        mesh=split,
        in_specs=placed,
        out_specs=(P(None, KV_TP), P(KV, "tp", None, None)),
        check_vma=False,
    )
```

profile of v0, /device:TPU:1, one launch (start us, length us, event | category | flops | bytes accessed | tf_op | source)
XLA Modules:
  0.0 214.8 jit_solution(3758858505448124838)
XLA Ops:
  7.2 0.0 copy-start
  7.2 0.0 copy-start.2
  7.2 0.0 copy-start.3
  7.2 0.0 copy-start.4
  7.2 0.0 copy-start.6
  7.2 0.0 all-gather.6.cloned.1.call-start
  7.3 0.8 copy.48
  8.1 1.6 pad_maximum_fusion
  9.7 0.0 all-gather.6.cloned.1.call-update
  9.7 1.2 copy.46
  10.9 1.0 reshape.175
  11.9 13.1 %all-to-all-start = ((bf16[64,2,1024]{2,1,0:T(2,128)(2,1)}), bf16[64,2,1024]{2,1,0:T(2,128)(2,1)S(1)}, u32[]{:S(2)}, u32[]{:S(2)}) async-start(bf16[64,2,1024]{2,1,0:T(2,128)(2,1)} %reshape.175), calls=%async_computation | async-start | bytes 524288 | tf_op jit(solution)/shard_map/all_to_all | solution.py:122
  25.1 0.0 all-gather.8.cloned.1.call-start
  25.1 0.0 copy-done.2
  25.2 0.0 copy-done.3
  25.2 0.0 copy-done.4
  25.3 0.0 copy-done.6
  25.3 7.0 %add_select_fusion = f32[8,4,128,128]{3,2,1,0:T(8,128)S(1)} fusion(f32[8,4,128,128]{3,2,1,0:T(8,128)} %param.20, f32[8,4,128]{2,1,0:T(4,128)S(1)} %get-tuple-element.34, f32[8,4,128]{2,1,0:T(4,128)S(1)} %get-tuple-element.30, f32[8,4,128]{2,1,0:T(4,128)S(1)} %get-tuple-element.32, f32[8,4,128]{2,1,0:T(4,128)S(1)} %get-tuple-element.29, ...), kind=kLoop, calls=%fused_computation.11 | loop fusion | flops 8388608 | bytes 4390944 | tf_op jit(solution)/shard_map/jit(_where)/select_n | solution.py:88
  32.4 0.0 copy-start.1
  32.4 6.9 %all-to-all-done = bf16[64,2,1024]{2,1,0:T(2,128)(2,1)S(1)} async-done(((bf16[64,2,1024]{2,1,0:T(2,128)(2,1)}), bf16[64,2,1024]{2,1,0:T(2,128)(2,1)S(1)}, u32[]{:S(2)}, u32[]{:S(2)}) %all-to-all-start) | async-done | bytes 262176 | tf_op jit(solution)/shard_map/all_to_all | solution.py:122
  39.3 0.3 reshape.176
  39.6 0.1 convert_bitcast_fusion
  39.7 1.6 copy.47
  41.3 1.6 reshape.160
  42.9 0.3 fusion.8
  43.2 64.3 %all-gather.6.cloned.1.call-done = bf16[4096,1537]{1,0:T(8,128)(2,1)} async-done(((bf16[64,1537]{1,0:T(8,128)(2,1)}), bf16[4096,1537]{1,0:T(8,128)(2,1)}) %all-gather.6.cloned.1.call-update) | async-done | bytes 12591120 | tf_op jit(solution)/shard_map/all_gather | solution.py:18
  107.5 1.6 convert_reduce_fusion
  109.1 5.7 %fusion = f32[32,1536]{1,0:T(8,128)S(1)} fusion(bf16[4096,1537]{1,0:T(8,128)(2,1)} %all-gather.6.cloned.1.call-done, f32[32,4096]{1,0:T(8,128)S(1)} %reshape.160, f32[4096]{0:T(1024)S(1)} %convert_reduce_fusion), kind=kOutput, calls=%fused_computation | convolution fusion | flops 402915328 | bytes 13320192 | tf_op jit(solution)/shard_map/dot_general | solution.py:127
  114.9 0.1 fusion.26
  115.2 1.5 fusion.6
  116.7 2.9 %fusion.21 = f32[8,4,1,128]{3,2,1,0:T(1,128)S(1)} fusion(f32[8,4,128,1]{2,3,1,0:T(1,128)S(1)} %bitcast.128, f32[8,4,128,128]{3,2,1,0:T(8,128)S(1)} %add_select_fusion, f32[8,4,128]{2,1,0:T(4,128)S(1)} %get-tuple-element.22, f32[8,4,128]{2,1,0:T(4,128)S(1)} %get-tuple-element.18, f32[8,4,128]{2,1,0:T(4,128)S(1)} %get-tuple-element.40, ...), kind=kOutput, calls=%fused_computation.30 | convolution fusion | flops 4194304 | bytes 2228224 | tf_op jit(solution)/shard_map/shk,shkv->shv/dot_general | solution.py:96
  119.6 4.7 %fusion.7 = f32[8,4,1,128]{3,2,1,0:T(1,128)S(1)} fusion(f32[8,4,128,1]{2,3,1,0:T(1,128)S(1)} %bitcast.127, f32[8,4,128]{2,1,0:T(4,128)S(1)} %get-tuple-element.21, f32[8,4,128]{2,1,0:T(4,128)S(1)} %get-tuple-element.17, f32[8,4,128]{2,1,0:T(4,128)S(1)} %get-tuple-element.41, f32[8,4,128,128]{3,2,1,0:T(8,128)S(1)} %add_select_fusion, ...), kind=kOutput, calls=%fused_computation.13 | convolution fusion | flops 5767168 | bytes 2277376 | tf_op jit(solution)/shard_map/shk,shkv->shv/dot_general | solution.py:96
  124.3 0.0 copy-done.1
  124.3 0.0 copy-start.5
  124.3 5.8 %fusion.2 = f32[8,4,1,128]{3,2,1,0:T(1,128)S(1)} fusion(f32[8,4,128,1]{2,3,1,0:T(1,128)S(1)} %bitcast.126, f32[8,4,128]{2,1,0:T(4,128)S(1)} %get-tuple-element.20, f32[8,4,128]{2,1,0:T(4,128)S(1)} %get-tuple-element.16, f32[8,4,128]{2,1,0:T(4,128)S(1)} %get-tuple-element.39, f32[8,4,128]{2,1,0:T(4,128)S(1)} %get-tuple-element.21, ...), kind=kOutput, calls=%fused_computation.4 | convolution fusion | flops 7340032 | bytes 2326528 | tf_op jit(solution)/shard_map/shk,shkv->shv/dot_general | solution.py:96
  130.1 0.1 multiply_reduce_fusion
  130.3 0.1 broadcast_multiply_fusion
  130.4 0.0 copy-done.5
  130.4 9.8 %all_gather.19 = bf16[4,32,512]{2,1,0:T(8,128)(2,1)} all-gather(bf16[1,32,512]{2,1,0:T(8,128)(2,1)S(1)} %multiply_convert_fusion.2), channel_id=1, replica_groups=mesh['kv_0'=8,'kv_1'=4,'kv_2'=2,'tp'=4] {'kv_1'}, dimensions={0}, use_global_device_ids=true | all-gather | bytes 163840 | tf_op jit(solution)/shard_map/all_gather | solution.py:35
  140.3 0.0 all-gather.8.cloned.1.call-update
  140.3 0.0 all-gather.10.cloned.1.call-start
  140.4 33.0 %all-gather.8.cloned.1.call-done = bf16[32,32,512]{2,1,0:T(8,128)(2,1)} async-done(((bf16[4,32,512]{2,1,0:T(8,128)(2,1)}), bf16[32,32,512]{2,1,0:T(8,128)(2,1)}) %all-gather.8.cloned.1.call-update) | async-done | bytes 1048592 | tf_op jit(solution)/shard_map/all_gather | solution.py:35
  173.3 0.0 all-gather.10.cloned.1.call-update
  173.4 21.9 %all-gather.10.cloned.1.call-done = bf16[16,4,32,512]{3,2,1,0:T(8,128)(2,1)} async-done(((bf16[8,4,32,512]{3,2,1,0:T(8,128)(2,1)}), bf16[16,4,32,512]{3,2,1,0:T(8,128)(2,1)}) %all-gather.10.cloned.1.call-update) | async-done | bytes 2097168 | tf_op jit(solution)/shard_map/all_gather | solution.py:35
  195.2 1.8 copy.57
  197.1 0.0 copy-done
  197.1 0.7 convolution_convert_fusion
  197.8 9.8 %all_to_all.18 = bf16[4,2048,16]{1,2,0:T(8,128)(2,1)S(1)} all-to-all(bf16[4,2048,16]{1,2,0:T(8,128)(2,1)S(1)} %bitcast.115), channel_id=1, replica_groups=mesh['kv_0'=8,'kv_1'=4,'kv_2'=2,'tp'=4] {'tp'}, dimensions={0} | all-to-all | bytes 524288 | tf_op jit(solution)/shard_map/all_to_all | solution.py:54
  207.6 0.7 reduce_sum.32
  (18 shorter events, 0.4 us)
Async XLA Ops:
  7.2 189.9 %copy-start = (bf16[512,64]{0,1:T(8,128)(2,1)S(1)}, bf16[512,64]{0,1:T(8,128)(2,1)}, u32[]{:S(2)}) copy-start(bf16[512,64]{0,1:T(8,128)(2,1)} %param.19) | copy-start | bytes 196612
  7.2 18.0 %copy-start.2 = (f32[8,4,512]{2,1,0:T(4,128)S(1)}, f32[8,4,512]{2,1,0:T(4,128)}, u32[]{:S(2)}) copy-start(f32[8,4,512]{2,1,0:T(4,128)} %param.21) | copy-start | bytes 196612
  7.2 18.0 %copy-start.3 = (bf16[8,4,512]{2,1,0:T(4,128)(2,1)S(1)}, bf16[8,4,512]{2,1,0:T(4,128)(2,1)}, u32[]{:S(2)}) copy-start(bf16[8,4,512]{2,1,0:T(4,128)(2,1)} %param.22) | copy-start | bytes 98308
  7.2 18.0 %copy-start.4 = (f32[512]{0:T(512)S(1)}, f32[512]{0:T(512)}, u32[]{:S(2)}) copy-start(f32[512]{0:T(512)} %param.17) | copy-start | bytes 6148
  7.2 18.1 %copy-start.6 = (s32[8]{0:T(128)S(1)}, s32[8]{0:T(128)}, u32[]{:S(2)}) copy-start(s32[8]{0:T(128)} %param.23) | copy-start | bytes 100
  7.2 100.3 %all-gather.6.cloned.1.call-start = ((), (), s32[]{:S(2)}) async-start(), calls=%async_computation.2 | async-start | bytes 13844480 | tf_op jit(solution)/shard_map/all_gather | solution.py:18
  11.9 27.3 %all-to-all-start = ((bf16[64,2,1024]{2,1,0:T(2,128)(2,1)}), bf16[64,2,1024]{2,1,0:T(2,128)(2,1)S(1)}, u32[]{:S(2)}, u32[]{:S(2)}) async-start(bf16[64,2,1024]{2,1,0:T(2,128)(2,1)} %reshape.175), calls=%async_computation | async-start | bytes 524288 | tf_op jit(solution)/shard_map/all_to_all | solution.py:122
  25.1 148.3 %all-gather.8.cloned.1.call-start = ((), (), s32[]{:S(2)}) async-start(), calls=%async_computation.3 | async-start | bytes 1179648 | tf_op jit(solution)/shard_map/all_gather | solution.py:35
  32.4 91.9 %copy-start.1 = (f32[8,4,128,128]{3,2,1,0:T(8,128)}, f32[8,4,128,128]{3,2,1,0:T(8,128)S(1)}, u32[]{:S(2)}) copy-start(f32[8,4,128,128]{3,2,1,0:T(8,128)S(1)} %add_select_fusion) | copy-start | bytes 6291460
  124.3 6.1 %copy-start.5 = (f32[512]{0:T(512)S(1)}, f32[512]{0:T(512)}, u32[]{:S(2)}) copy-start(f32[512]{0:T(512)} %param.18) | copy-start | bytes 6148
  140.3 54.9 %all-gather.10.cloned.1.call-start = ((), (), s32[]{:S(2)}) async-start(), calls=%async_computation.4 | async-start | bytes 3145728 | tf_op jit(solution)/shard_map/all_gather | solution.py:35
Sparse Core Ops, SparseCore 0:
  10.8 96.7 all-gather.5
  140.4 32.8 all-gather.7
  175.2 20.0 all-gather.9
where the time goes:
time: 215 us
  waiting for transfers between devices  126 us (59%)
  matrix products  21.4 us (10%)
  blocking collectives  19.6 us (9%)
  between operations  14 us (7%)
  starting transfers between devices  13.3 us (6%)
  other arithmetic  11.7 us (5%)
  local copies, waits for them, and re-layouts  8.64 us (4%)
    all_gather x1, waiting for transfers between devices, side_by_side(): out, at, outs = (lax.all_gather(both, axis, axis=dim, tiled=True), 0, [])  64.3 us
    all_gather x2, waiting for transfers between devices, gather_in_order(): blocks = lax.all_gather(blocks, axes[k])  54.9 us
    dot_general x4, matrix products, recurrence(): results.append(jnp.einsum('shk,shkv->shv', queries[:, position], carried))  14.9 us
    all_to_all x1, starting transfers between devices, body(): lax.all_to_all(inputs, KV, split_axis=0, concat_axis=1, tiled=True)  13.1 us
    all_gather x1, blocking collectives, gather_in_order(): blocks = lax.all_gather(blocks, axes[k])  9.85 us
    all_to_all x1, blocking collectives, sum_at_owner(): blocks = lax.all_to_all(cut_along(array, dim, size), axis, 0, 0, tiled=True)  9.77 us
    select_n x1, other arithmetic, recurrence(): carried = jnp.where(taken_up, folded, carried)  7.02 us
    all_to_all x1, waiting for transfers between devices, body(): lax.all_to_all(inputs, KV, split_axis=0, concat_axis=1, tiled=True)  6.88 us
  transfers between devices with their start and end apart: 4, of which 4 were waited for; matrix products, arithmetic and copies ran while one was open for 6% of the time, Pallas kernels for 0%

commit v1 on v0

v1 whole, which is shorter than its diff:
```python
import functools

import jax
import jax.numpy as jnp
from jax import lax
from jax.experimental import pallas as pl
from jax.experimental.pallas import tpu as pltpu
from jax.sharding import Mesh
from jax.sharding import PartitionSpec as P

KV = ("kv_0", "kv_1", "kv_2")
KV_TP = ("kv_0", "kv_1", "kv_2", "tp")
MESH_ID = pl.DeviceIdType.MESH
EPSILON = 1e-06
F32 = jnp.float32
BF16 = jnp.bfloat16

D = 4096
Z, Y, C, X = 8, 4, 2, 4
G = Y * C
FEATS = 64
OWN = 32
SET = Z * OWN
TOKENS = 2048
HEADS = 4
HEAD = 128
COLS = HEADS * HEAD
SEQS = 8
STEPS = 4
CHUNKS = 3
UP, DOWN = 0, 1
HOPS = ((4, 3), (3, 4), (4, 3))


def kernel(
    x_hbm,
    gain_ref,
    wq_hbm,
    wf_hbm,
    wv_hbm,
    wo_hbm,
    floor_ref,
    head_gain_ref,
    prior_hbm,
    prev_gate_ref,
    prev_value_ref,
    accepted_ref,
    out_ref,
    base_hbm,
    x_raw,
    x_send,
    x_all,
    sq_send,
    sq_all,
    sq_mine,
    sq_z,
    w_all,
    state,
    base_low,
    part,
    ring_send,
    ring_recv,
    normed_all,
    cross_send,
    cross_recv,
    final_send,
    final_recv,
    local_sem,
    x_sems,
    sq_sems,
    sqz_sems,
    w_sems,
    ring_sems,
    normed_sems,
    cross_sems,
    final_sems,
):
    z = lax.axis_index("kv_0")
    y = lax.axis_index("kv_1")
    c = lax.axis_index("kv_2")
    x = lax.axis_index("tp")
    g = y * C + c

    def at_z(step):
        return lax.rem(z + (step + Z), Z)

    def at_y(step):
        return lax.rem(y + (step + Y), Y)

    def at_x(step):
        return lax.rem(x + (step + X), X)

    sib = 1 - c
    above, below = at_y(1), at_y(-1)
    group_steps = [(dy, dc) for dy in range(Y) for dc in range(C) if dy or dc]

    def group_peer(dy, dc):
        return at_y(dy), (sib if dc else c)

    x_load = pltpu.make_async_copy(x_hbm, x_raw, local_sem.at[0])
    x_load.start()
    w_loads = []
    for j, src in enumerate((wq_hbm, wf_hbm, wv_hbm, wo_hbm)):
        load = pltpu.make_async_copy(src, w_all.at[j, g], local_sem.at[1 + j])
        load.start()
        w_loads.append(load)
    prior_load = pltpu.make_async_copy(prior_hbm, state, local_sem.at[5])
    prior_load.start()

    barrier = pltpu.get_barrier_semaphore()
    peers = []
    for dy, dc in group_steps:
        py, pc = group_peer(dy, dc)
        peers.append((z, py, pc, x))
    for dz in range(1, Z):
        peers.append((at_z(dz), y, c, x))
    for dx in range(1, X):
        peers.append((z, y, c, at_x(dx)))
    for peer in peers:
        pl.semaphore_signal(barrier, inc=1, device_id=peer, device_id_type=MESH_ID)

    gain_col = jnp.transpose(jnp.broadcast_to(gain_ref[...].astype(F32), (HEAD, FEATS)))
    lane_block = lax.broadcasted_iota(jnp.int32, (FEATS, HEAD), 1) // OWN
    x_load.wait()
    for peer in range(G):
        for half in range(2):
            tile = None
            for k in range(4):
                zz = half * 4 + k
                src = x_raw[:, pl.ds(zz * 256 + (peer // 4) * 128, 128)].astype(F32)
                shift = ((k - peer % 4) * OWN) % 128
                if shift:
                    src = pltpu.roll(src, shift, 1)
                tile = src if tile is None else jnp.where(lane_block == k, src, tile)
            lanes = pl.ds(half * 128, 128)
            sq_send[peer, :, lanes] = jnp.sum(tile * tile, axis=0, keepdims=True)
            x_send[peer, :, lanes] = (tile * gain_col).astype(BF16)

    pl.semaphore_wait(barrier, len(peers))

    def remote(src, dst, sems, index, peer):
        return pltpu.make_async_remote_copy(
            src_ref=src,
            dst_ref=dst,
            send_sem=sems.at[0, index],
            recv_sem=sems.at[1, index],
            device_id=peer,
            device_id_type=MESH_ID,
        )

    started = []

    def go(copy):
        copy.start()
        started.append(copy)
        return copy

    x_copies, sq_copies = [], []
    for i, (dy, dc) in enumerate(group_steps):
        py, pc = group_peer(dy, dc)
        pg = py * C + pc
        peer = (z, py, pc, x)
        x_copies.append(go(remote(x_send.at[pg], x_all.at[g], x_sems, i, peer)))
        sq_copies.append(go(remote(sq_send.at[pg], sq_all.at[g], sq_sems, i, peer)))
    x_all[g] = x_send[g]
    sq_all[g] = sq_send[g]

    W = []
    for j in range(4):
        w_loads[j].wait()
        own = w_all.at[j, g]
        W.append(
            {
                "up": go(remote(own, own, w_sems, j * 8 + 0, (z, above, c, x))),
                "down": go(remote(own, own, w_sems, j * 8 + 1, (z, below, c, x))),
                "sib0": go(remote(own, own, w_sems, j * 8 + 2, (z, y, sib, x))),
            }
        )
    half = FEATS // 2
    g_below, g_above, g_far = below * C + c, above * C + c, at_y(2) * C + c

    def forward(j):
        W[j]["up"].wait_recv()
        piece = w_all.at[j, g_below, pl.ds(0, half)]
        W[j]["up2"] = go(remote(piece, piece, w_sems, j * 8 + 3, (z, above, c, x)))
        block = w_all.at[j, g_below]
        W[j]["sib1"] = go(remote(block, block, w_sems, j * 8 + 4, (z, y, sib, x)))
        W[j]["down"].wait_recv()
        piece = w_all.at[j, g_above, pl.ds(half, half)]
        W[j]["down2"] = go(remote(piece, piece, w_sems, j * 8 + 5, (z, below, c, x)))
        block = w_all.at[j, g_above]
        W[j]["sib2"] = go(remote(block, block, w_sems, j * 8 + 6, (z, y, sib, x)))

    def forward_far(j):
        W[j]["up2"].wait_recv()
        W[j]["down2"].wait_recv()
        block = w_all.at[j, g_far]
        W[j]["sib3"] = go(remote(block, block, w_sems, j * 8 + 7, (z, y, sib, x)))

    def complete(j):
        for k in range(4):
            W[j]["sib%d" % k].wait_recv()

    prior_load.wait()
    position = lax.broadcasted_iota(jnp.int32, (STEPS, COLS), 0)
    decays, keys_old, values_old = [], [], []
    for s in range(SEQS):
        taken = position < accepted_ref[s]
        gate = jnp.where(taken, prev_gate_ref[s], 1.0)
        key = 1.0 - gate
        after = jnp.ones((1, COLS), F32)
        rows = [None] * STEPS
        for j in reversed(range(STEPS)):
            rows[j] = key[j : j + 1] * after
            after = after * gate[j : j + 1]
        decays.append(after)
        keys_old.append(jnp.concatenate(rows, axis=0))
        values_old.append(prev_value_ref[s].astype(F32))
    for h in range(HEADS):
        cols = slice(h * HEAD, (h + 1) * HEAD)
        decay_cols = jnp.transpose(
            jnp.concatenate([decays[s][:, cols] for s in range(SEQS)], axis=0)
        )
        for s in range(SEQS):
            added = lax.dot_general(
                keys_old[s][:, cols],
                values_old[s][:, cols],
                (((0,), (0,)), ((), ())),
                precision=lax.Precision.HIGHEST,
                preferred_element_type=F32,
            )
            new = state[s, h] * decay_cols[:, s : s + 1] + added
            state[s, h] = new
            base_low[s, h] = new.astype(BF16)
    base_store = pltpu.make_async_copy(state, base_hbm, local_sem.at[6])
    base_store.start()

    def squares_out():
        for copy in sq_copies:
            copy.wait_recv()
        total = sq_all[0]
        for k in range(1, G):
            total = total + sq_all[k]
        sq_mine[...] = total
        copies = []
        for dz in range(1, Z):
            peer = (at_z(dz), y, c, x)
            copies.append(go(remote(sq_mine, sq_z.at[z], sqz_sems, dz - 1, peer)))
        sq_z[z] = total
        return copies

    lefts = {}

    def multiply(j):
        if "x" not in lefts:
            for copy in x_copies:
                copy.wait_recv()
            lefts["x"] = jnp.transpose(x_all[...].reshape(G * FEATS, SET))
        product = jnp.dot(
            lefts["x"], w_all[j].reshape(G * FEATS, COLS), preferred_element_type=F32
        )
        part[j] = product.reshape(Z, OWN, COLS)

    ring = {}

    def ring_step(j, step):
        for way in (UP, DOWN):
            hops = HOPS[j][way]
            if step > hops:
                continue
            sign = 1 if way == UP else -1
            value = part[j, at_z(sign * (hops - step + 1))]
            if step > 1:
                ring[j, way, step - 1].wait_recv()
                value = value + ring_recv[j, way, step - 2].astype(F32)
            ring_send[j, way, step - 1] = value.astype(BF16)
            ring[j, way, step] = go(
                remote(
                    ring_send.at[j, way, step - 1],
                    ring_recv.at[j, way, step - 1],
                    ring_sems,
                    (j * 2 + way) * 4 + step - 1,
                    (at_z(sign), y, c, x),
                )
            )

    def ring_end(j):
        value = part[j, z]
        for way in (UP, DOWN):
            ring[j, way, HOPS[j][way]].wait_recv()
            value = value + ring_recv[j, way, HOPS[j][way] - 1].astype(F32)
        return value

    forward(0)
    forward(1)
    forward_far(0)
    sqz_copies = squares_out()
    complete(0)
    multiply(0)
    ring_step(0, 1)
    forward(2)
    forward_far(1)
    complete(1)
    multiply(1)
    ring_step(1, 1)
    forward(3)
    ring_step(0, 2)
    forward_far(2)
    complete(2)
    multiply(2)
    ring_step(2, 1)
    ring_step(1, 2)
    ring_step(0, 3)
    forward_far(3)
    ring_step(2, 2)
    ring_step(1, 3)
    ring_step(0, 4)
    ring_step(2, 3)
    ring_step(1, 4)
    ring_step(2, 4)
    complete(3)

    for copy in sqz_copies:
        copy.wait_recv()
    squares = sq_z[0]
    for k in range(1, Z):
        squares = squares + sq_z[k]
    token = lax.broadcasted_iota(jnp.int32, (OWN, SET), 0) + z * OWN
    lane = lax.broadcasted_iota(jnp.int32, (OWN, SET), 1)
    own_squares = jnp.sum(
        jnp.where(lane == token, jnp.broadcast_to(squares, (OWN, SET)), 0.0),
        axis=1,
        keepdims=True,
    )
    rscale = lax.rsqrt(own_squares / D + EPSILON)

    query_pre = ring_end(0) * rscale
    forget_pre = ring_end(1) * rscale
    value_pre = ring_end(2) * rscale

    row = lax.broadcasted_iota(jnp.int32, (OWN, HEAD), 0)
    when = lax.rem(row, STEPS)
    first_seq = lax.broadcasted_iota(jnp.int32, (8, HEAD), 0) < STEPS
    for h in range(HEADS):
        cols = slice(h * HEAD, (h + 1) * HEAD)
        floor = floor_ref[h : h + 1, :]
        gate = floor + (1.0 - floor) * jax.nn.sigmoid(forget_pre[:, cols])
        key = 1.0 - gate
        pre = query_pre[:, cols]
        query = pre * jax.nn.sigmoid(pre)
        value = value_pre[:, cols]
        decayed = query
        result = jnp.sum(query * key, axis=1, keepdims=True) * value
        for back in range(1, STEPS):
            gate_back = gate if back == 1 else pltpu.roll(gate, back - 1, 0)
            decayed = decayed * (
                gate_back if back == 1 else jnp.where(when >= back - 1, gate_back, 1.0)
            )
            weight = jnp.sum(
                jnp.where(when >= back, decayed * pltpu.roll(key, back, 0), 0.0),
                axis=1,
                keepdims=True,
            )
            result = result + weight * pltpu.roll(value, back, 0)
        decayed = decayed * jnp.where(when >= STEPS - 1, pltpu.roll(gate, STEPS - 1, 0), 1.0)
        low = decayed.astype(BF16)
        carried = []
        for pair in range(SEQS // 2):
            rows = low[pair * 8 : pair * 8 + 8]
            one = jnp.dot(rows, base_low[2 * pair, h], preferred_element_type=F32)
            two = jnp.dot(rows, base_low[2 * pair + 1, h], preferred_element_type=F32)
            carried.append(jnp.where(first_seq, one, two))
        result = result + jnp.concatenate(carried, axis=0)
        mean = jnp.sum(result * result, axis=1, keepdims=True) / HEAD
        normed = result * lax.rsqrt(mean + EPSILON) * head_gain_ref[h : h + 1, :]
        normed_all[z, :, cols] = normed.astype(BF16)

    copies = []
    for i, dz in enumerate((4, 3, 5, 2, 6, 1, 7)):
        slot = normed_all.at[z]
        copies.append(go(remote(slot, slot, normed_sems, i, (at_z(dz), y, c, x))))
    for copy in copies:
        copy.wait_recv()

    product = lax.dot_general(
        w_all[3].reshape(G * FEATS, COLS),
        normed_all[...].reshape(SET, COLS),
        (((1,), (1,)), ((), ())),
        preferred_element_type=F32,
    )
    pieces = product.astype(BF16).reshape(G, X, FEATS // X, SET)
    for k in range(X):
        cross_send[k] = pieces[:, k]
    copies = []
    for dx in (2, 1, 3):
        to = at_x(dx)
        copies.append(
            go(remote(cross_send.at[to], cross_recv.at[dx - 1], cross_sems, dx - 1, (z, y, c, to)))
        )
    total = cross_send[x].astype(F32)
    for dx, copy in zip((2, 1, 3), copies):
        copy.wait_recv()
        total = total + cross_recv[dx - 1].astype(F32)
    final_send[...] = total.astype(BF16)
    copies = []
    for i, (dy, dc) in enumerate(group_steps):
        py, pc = group_peer(dy, dc)
        pg = py * C + pc
        peer = (z, py, pc, x)
        copies.append(go(remote(final_send.at[pg], final_recv.at[g], final_sems, i, peer)))
    final_recv[g] = final_send[g]
    for copy in copies:
        copy.wait_recv()

    rows_out = FEATS // X
    lane_block = lax.broadcasted_iota(jnp.int32, (rows_out, HEAD), 1) // OWN
    for zz in range(Z):
        for half_g in range(2):
            tile = None
            for k in range(4):
                src = final_recv[half_g * 4 + k, :, pl.ds((zz // 4) * 128, 128)].astype(F32)
                shift = ((k - zz % 4) * OWN) % 128
                if shift:
                    src = pltpu.roll(src, shift, 1)
                tile = src if tile is None else jnp.where(lane_block == k, src, tile)
            out_ref[:, pl.ds(zz * 256 + half_g * 128, 128)] = tile.astype(BF16)

    for copy in started:
        copy.wait_send()
    base_store.wait()


def fused(*args):
    any_space = pl.BlockSpec(memory_space=pl.ANY)
    vmem = pl.BlockSpec(memory_space=pltpu.VMEM)
    smem = pl.BlockSpec(memory_space=pltpu.SMEM)
    dma = lambda n: pltpu.SemaphoreType.DMA((2, n))
    return pl.pallas_call(
        kernel,
        out_shape=(
            jax.ShapeDtypeStruct((FEATS // X, TOKENS), BF16),
            jax.ShapeDtypeStruct((SEQS, HEADS, HEAD, HEAD), F32),
        ),
        in_specs=[any_space, vmem] + [any_space] * 4 + [vmem, vmem, any_space, vmem, vmem, smem],
        out_specs=(vmem, any_space),
        scratch_shapes=[
            pltpu.VMEM((FEATS, TOKENS), BF16),
            pltpu.VMEM((G, FEATS, SET), BF16),
            pltpu.VMEM((G, FEATS, SET), BF16),
            pltpu.VMEM((G, 1, SET), F32),
            pltpu.VMEM((G, 1, SET), F32),
            pltpu.VMEM((1, SET), F32),
            pltpu.VMEM((Z, 1, SET), F32),
            pltpu.VMEM((4, G, FEATS, COLS), BF16),
            pltpu.VMEM((SEQS, HEADS, HEAD, HEAD), F32),
            pltpu.VMEM((SEQS, HEADS, HEAD, HEAD), BF16),
            pltpu.VMEM((CHUNKS, Z, OWN, COLS), F32),
            pltpu.VMEM((CHUNKS, 2, 4, OWN, COLS), BF16),
            pltpu.VMEM((CHUNKS, 2, 4, OWN, COLS), BF16),
            pltpu.VMEM((Z, OWN, COLS), BF16),
            pltpu.VMEM((X, G, FEATS // X, SET), BF16),
            pltpu.VMEM((X - 1, G, FEATS // X, SET), BF16),
            pltpu.VMEM((G, FEATS // X, SET), BF16),
            pltpu.VMEM((G, FEATS // X, SET), BF16),
            pltpu.SemaphoreType.DMA((7,)),
            dma(G - 1),
            dma(G - 1),
            dma(Z - 1),
            dma(32),
            dma(CHUNKS * 8),
            dma(Z - 1),
            dma(X - 1),
            dma(G - 1),
        ],
        compiler_params=pltpu.CompilerParams(collective_id=0, has_side_effects=True),
    )(*args)


def body(
    inputs,
    norm_gain,
    w_query,
    w_forget,
    w_value,
    lower_bound,
    head_gain,
    w_out,
    prior_state,
    prev_forget,
    prev_values,
    accepted,
):
    mixed, base_state = fused(
        inputs.T,
        norm_gain.reshape(1, FEATS),
        w_query,
        w_forget,
        w_value,
        w_out.T,
        lower_bound.reshape(HEADS, HEAD),
        head_gain.reshape(HEADS, HEAD),
        prior_state,
        prev_forget,
        prev_values,
        accepted,
    )
    return (mixed.T, base_state)


def solution(mesh):
    split = Mesh(mesh.devices.reshape(Z, Y, C, X), KV_TP)
    placed = (
        P(None, KV),
        P(KV),
        P(KV, "tp"),
        P(KV, "tp"),
        P(KV, "tp"),
        P("tp"),
        P("tp"),
        P("tp", KV),
        P(KV, "tp", None, None),
        P(KV, None, "tp"),
        P(KV, None, "tp"),
        P(KV),
    )
    return jax.shard_map(
        body,
        mesh=split,
        in_specs=placed,
        out_specs=(P(None, KV_TP), P(KV, "tp", None, None)),
        check_vma=False,
    )
```

time: 215 us -> 65.5 us (0.30)
  waiting for transfers between devices: 126 us -> 0 us
  Pallas kernels: 0 us -> 60 us
  matrix products: 21.4 us -> 0 us
  blocking collectives: 19.6 us -> 0 us
  between operations: 14 us -> 0.64 us
  starting transfers between devices: 13.3 us -> 0 us
  other arithmetic: 11.7 us -> 0 us
  local copies, waits for them, and re-layouts: 8.64 us -> 4.61 us
    all_gather x3 -> x0, waiting for transfers between devices: 119 us -> none  [the longest x1 64.3 us: side_by_side(): out, at, outs = (lax.all_gather(both, axis, axis=dim, tiled=True), 0, [])]
    pallas_call x0 -> x1, Pallas kernels: none -> 60 us  [fused(): pl.pallas_call(kernel, out_shape=(jax.ShapeDtypeStruct((FEATS // X, TOKEN...]
    dot_general x6 -> x0, matrix products: 21.4 us -> none  [the longest x4 14.9 us: recurrence(): results.append(jnp.einsum('shk,shkv->shv', queries[:, position], carried))]
    all_to_all x1 -> x0, starting transfers between devices: 13.1 us -> none  [body(): lax.all_to_all(inputs, KV, split_axis=0, concat_axis=1, tiled=True)]
    all_gather x1 -> x0, blocking collectives: 9.85 us -> none  [gather_in_order(): blocks = lax.all_gather(blocks, axes[k])]
    all_to_all x1 -> x0, blocking collectives: 9.77 us -> none  [sum_at_owner(): blocks = lax.all_to_all(cut_along(array, dim, size), axis, 0, 0, tiled=True)]
    select_n x1 -> x0, other arithmetic: 7.02 us -> none  [recurrence(): carried = jnp.where(taken_up, folded, carried)]
    all_to_all x1 -> x0, waiting for transfers between devices: 6.88 us -> none  [body(): lax.all_to_all(inputs, KV, split_axis=0, concat_axis=1, tiled=True)]
  transfers between devices with their start and end apart: 4 -> 0, of which waited for: 4 -> 0; matrix products, arithmetic and copies ran while one was open for 6% -> 0% of each run, Pallas kernels for 0% -> 0%
where the time goes in v1:
time: 65.5 us; the launch traced here: 65.3 us
  Pallas kernels  60 us (92%)
  local copies, waits for them, and re-layouts  4.61 us (7%)
    pallas_call x1, Pallas kernels, fused(): pl.pallas_call(kernel, out_shape=(jax.ShapeDtypeStruct((FEATS // X, TOKEN...  60 us
    unnamed x2, local copies, waits for them, and re-layouts  4.61 us

profile of v1, /device:TPU:1, one launch (start us, length us, event | category | flops | bytes accessed | tf_op | source)
XLA Modules:
  0.0 65.3 jit_solution(7554701590997017467)
XLA Ops:
  0.6 60.0 %shard_map.131 = (bf16[16,2048]{1,0:T(8,128)(2,1)}, f32[8,4,128,128]{3,2,1,0:T(8,128)}) custom-call(bf16[64,2048]{1,0:T(8,128)(2,1)} %bitcast.6, bf16[1,64]{1,0:T(2,128)(2,1)} %bitcast.11, bf16[64,512]{1,0:T(8,128)(2,1)} %wq_hbm.1, bf16[64,512]{1,0:T(8,128)(2,1)} %wf_hbm.1, bf16[64,512]{1,0:T(8,128)(2,1)} %wv_hbm.1, bf16[64,512]{1,0:T(8,128)(2,1)} %bitcast.7, ...), custom_call_target="tpu_custom_call" | custom-call | tf_op jit(solution)/shard_map/pallas_call | solution.py:438
  60.6 1.5 %copy.16 = bf16[2048,16]{0,1:T(8,128)(2,1)} copy(bf16[2048,16]{0,1:T(8,128)(2,1)} %bitcast.8) | data formatting | bytes 131072
  62.1 3.1 %copy.17 = f32[8,4,128,128]{3,2,1,0:T(8,128)} copy(f32[8,4,128,128]{3,2,1,0:T(8,128)} %get-tuple-element.9) | data formatting | bytes 4194304

commit v2 on v1

v2 whole, which is shorter than its diff:
```python
import functools

import jax
import jax.numpy as jnp
from jax import lax
from jax.experimental import pallas as pl
from jax.experimental.pallas import tpu as pltpu
from jax.sharding import Mesh
from jax.sharding import PartitionSpec as P

KV = ("kv_0", "kv_1", "kv_2")
KV_TP = ("kv_0", "kv_1", "kv_2", "tp")
MESH_ID = pl.DeviceIdType.MESH
EPSILON = 1e-06
F32 = jnp.float32
BF16 = jnp.bfloat16

D = 4096
Z, Y, C, X = 8, 4, 2, 4
G = Y * C
FEATS = 64
OWN = 32
SET = Z * OWN
TOKENS = 2048
HEADS = 4
HEAD = 128
COLS = HEADS * HEAD
SEQS = 8
STEPS = 4
UP, DOWN = 0, 1
WIDE = 3 * HEAD
HOPS = ((4, 3), (3, 4), (4, 3), (3, 4))
MERGES = {4: ((4, 3), (2, 1)), 3: ((3, 2), (None, 1))}


def kernel(
    x_hbm,
    gain_ref,
    wq_hbm,
    wf_hbm,
    wv_hbm,
    wo_hbm,
    floor_ref,
    head_gain_ref,
    prior_hbm,
    prev_gate_ref,
    prev_value_ref,
    accepted_ref,
    out_ref,
    base_ref,
    x_raw,
    x_send,
    x_all,
    sq_send,
    sq_all,
    sq_mine,
    sq_z,
    w_all,
    wo_all,
    base_low,
    part,
    first_send,
    first_recv,
    second_send,
    second_recv,
    normed_all,
    final_send,
    final_recv,
    local_sem,
    x_sems,
    sq_sems,
    sqz_sems,
    w_sems,
    first_sems,
    second_sems,
    normed_sems,
    final_sems,
):
    z = lax.axis_index("kv_0")
    y = lax.axis_index("kv_1")
    c = lax.axis_index("kv_2")
    x = lax.axis_index("tp")
    g = y * C + c

    def at_z(step):
        return lax.rem(z + (step + Z), Z)

    def at_y(step):
        return lax.rem(y + (step + Y), Y)

    def at_x(step):
        return lax.rem(x + (step + X), X)

    sib = 1 - c
    group_steps = [(2, 0), (2, 1), (1, 0), (1, 1), (3, 0), (3, 1), (0, 1)]

    def group_peer(dy, dc):
        return at_y(dy), (sib if dc else c)

    barrier = pltpu.get_barrier_semaphore()
    peers = [(at_z(dz), y, c, x) for dz in (4, 3, 5, 2, 6, 1, 7)]
    for dy, dc in group_steps:
        py, pc = group_peer(dy, dc)
        peers.append((z, py, pc, x))
    for dx in range(1, X):
        peers.append((z, y, c, at_x(dx)))
    for peer in peers:
        pl.semaphore_signal(barrier, inc=1, device_id=peer, device_id_type=MESH_ID)

    x_load = pltpu.make_async_copy(x_hbm, x_raw, local_sem.at[0])
    x_load.start()
    w_loads = []
    for h in range(HEADS):
        loads = []
        for k, src in enumerate((wq_hbm, wf_hbm, wv_hbm)):
            load = pltpu.make_async_copy(
                src.at[:, pl.ds(h * HEAD, HEAD)],
                w_all.at[h, g, :, pl.ds(k * HEAD, HEAD)],
                local_sem.at[3 + h * 3 + k],
            )
            load.start()
            loads.append(load)
        w_loads.append(loads)
    wo_load = pltpu.make_async_copy(wo_hbm, wo_all.at[g], local_sem.at[1])
    wo_load.start()
    w_loads.append([wo_load])
    prior_load = pltpu.make_async_copy(prior_hbm, base_ref, local_sem.at[2])
    prior_load.start()

    gain_col = jnp.transpose(jnp.broadcast_to(gain_ref[...].astype(F32), (HEAD, FEATS)))
    lane_block = lax.broadcasted_iota(jnp.int32, (FEATS, HEAD), 1) // OWN
    x_load.wait()
    for peer in range(G):
        for half in range(2):
            tile = None
            for k in range(4):
                zz = half * 4 + k
                src = x_raw[:, pl.ds(zz * 256 + (peer // 4) * 128, 128)].astype(F32)
                shift = ((k - peer % 4) * OWN) % 128
                if shift:
                    src = pltpu.roll(src, shift, 1)
                tile = src if tile is None else jnp.where(lane_block == k, src, tile)
            lanes = pl.ds(half * 128, 128)
            sq_send[peer, :, lanes] = jnp.sum(tile * tile, axis=0, keepdims=True)
            x_send[peer, :, lanes] = (tile * gain_col).astype(BF16)

    pl.semaphore_wait(barrier, len(peers))

    def remote(src, dst, sems, index, peer):
        return pltpu.make_async_remote_copy(
            src_ref=src,
            dst_ref=dst,
            send_sem=sems.at[0, index],
            recv_sem=sems.at[1, index],
            device_id=peer,
            device_id_type=MESH_ID,
        )

    started = []

    def go(copy):
        copy.start()
        started.append(copy)
        return copy

    W = [{} for _ in range(HEADS + 1)]

    def w_slot(j, member):
        return w_all.at[j, member] if j < HEADS else wo_all.at[member]

    def w_out(j):
        for load in w_loads[j]:
            load.wait()
        own = w_slot(j, g)
        for i, dy in enumerate((2, 1, 3)):
            W[j][dy] = go(remote(own, own, w_sems, j * 7 + i, (z, at_y(dy), c, x)))
        W[j]["sib", 0] = go(remote(own, own, w_sems, j * 7 + 3, (z, y, sib, x)))

    def w_forward(j):
        for i, dy in enumerate((1, 3, 2)):
            W[j][dy].wait_recv()
            block = w_slot(j, at_y(-dy) * C + c)
            W[j]["sib", dy] = go(remote(block, block, w_sems, j * 7 + 4 + i, (z, y, sib, x)))

    def w_complete(j):
        for dy in (0, 1, 3, 2):
            W[j]["sib", dy].wait_recv()

    w_out(0)
    x_copies, sq_copies = [], []
    for i, (dy, dc) in enumerate(group_steps):
        py, pc = group_peer(dy, dc)
        pg = py * C + pc
        peer = (z, py, pc, x)
        x_copies.append(go(remote(x_send.at[pg], x_all.at[g], x_sems, i, peer)))
        sq_copies.append(go(remote(sq_send.at[pg], sq_all.at[g], sq_sems, i, peer)))
    for j in range(1, HEADS + 1):
        w_out(j)
    x_all[g] = x_send[g]
    sq_all[g] = sq_send[g]

    prior_load.wait()
    position = lax.broadcasted_iota(jnp.int32, (STEPS, COLS), 0)
    decays, keys_old, values_old = [], [], []
    for s in range(SEQS):
        taken = position < accepted_ref[s]
        gate = jnp.where(taken, prev_gate_ref[s], 1.0)
        key = 1.0 - gate
        after = jnp.ones((1, COLS), F32)
        rows = [None] * STEPS
        for j in reversed(range(STEPS)):
            rows[j] = key[j : j + 1] * after
            after = after * gate[j : j + 1]
        decays.append(after)
        keys_old.append(jnp.concatenate(rows, axis=0))
        values_old.append(prev_value_ref[s].astype(F32))
    for h in range(HEADS):
        cols = slice(h * HEAD, (h + 1) * HEAD)
        decay_cols = jnp.transpose(
            jnp.concatenate([decays[s][:, cols] for s in range(SEQS)], axis=0)
        )
        for s in range(SEQS):
            added = lax.dot_general(
                keys_old[s][:, cols],
                values_old[s][:, cols],
                (((0,), (0,)), ((), ())),
                precision=lax.Precision.HIGHEST,
                preferred_element_type=F32,
            )
            new = base_ref[s, h] * decay_cols[:, s : s + 1] + added
            base_ref[s, h] = new
            base_low[s, h] = new.astype(BF16)

    def squares_out():
        for copy in sq_copies:
            copy.wait_recv()
        total = sq_all[0]
        for k in range(1, G):
            total = total + sq_all[k]
        sq_mine[...] = total
        copies = []
        for dz in range(1, Z):
            peer = (at_z(dz), y, c, x)
            copies.append(go(remote(sq_mine, sq_z.at[z], sqz_sems, dz - 1, peer)))
        sq_z[z] = total
        return copies

    def token_scale(copies):
        for copy in copies:
            copy.wait_recv()
        squares = sq_z[0]
        for k in range(1, Z):
            squares = squares + sq_z[k]
        token = lax.broadcasted_iota(jnp.int32, (OWN, SET), 0) + z * OWN
        lane = lax.broadcasted_iota(jnp.int32, (OWN, SET), 1)
        own_squares = jnp.sum(
            jnp.where(lane == token, jnp.broadcast_to(squares, (OWN, SET)), 0.0),
            axis=1,
            keepdims=True,
        )
        return lax.rsqrt(own_squares / D + EPSILON)

    first, second = {}, {}

    def multiply(j, left):
        product = jnp.dot(left, w_all[j].reshape(G * FEATS, WIDE), preferred_element_type=F32)
        part[j] = product.reshape(Z, OWN, WIDE)
        for way, sign in ((UP, 1), (DOWN, -1)):
            for m, (far, near) in enumerate(MERGES[HOPS[j][way]]):
                index = (j * 2 + way) * 2 + m
                if far is None:
                    second_send[j, way, m] = part[j, at_z(sign * near)].astype(BF16)
                    src, dst, sems = second_send.at[j, way, m], second_recv.at[j, way, m], second_sems
                    second[j, way, m] = go(
                        remote(src, dst, sems, index, (at_z(sign * near), y, c, x))
                    )
                else:
                    first_send[j, way, m] = part[j, at_z(sign * far)].astype(BF16)
                    src, dst, sems = first_send.at[j, way, m], first_recv.at[j, way, m], first_sems
                    first[j, way, m] = go(remote(src, dst, sems, index, (at_z(sign), y, c, x)))

    def merge(j):
        for m in range(2):
            for way, sign in ((UP, 1), (DOWN, -1)):
                far, near = MERGES[HOPS[j][way]][m]
                if far is None:
                    continue
                first[j, way, m].wait_recv()
                value = part[j, at_z(sign * near)] + first_recv[j, way, m].astype(F32)
                second_send[j, way, m] = value.astype(BF16)
                src, dst = second_send.at[j, way, m], second_recv.at[j, way, m]
                index = (j * 2 + way) * 2 + m
                second[j, way, m] = go(
                    remote(src, dst, second_sems, index, (at_z(sign * near), y, c, x))
                )

    row = lax.broadcasted_iota(jnp.int32, (OWN, HEAD), 0)
    when = lax.rem(row, STEPS)
    first_seq = lax.broadcasted_iota(jnp.int32, (8, HEAD), 0) < STEPS
    normed_copies = []

    def recur(h, rscale):
        total = part[h, z]
        for way in (UP, DOWN):
            for m in range(2):
                second[h, way, m].wait_recv()
                total = total + second_recv[h, way, m].astype(F32)
        total = total * rscale
        floor = floor_ref[h : h + 1, :]
        gate = floor + (1.0 - floor) * jax.nn.sigmoid(total[:, HEAD : 2 * HEAD])
        key = 1.0 - gate
        pre = total[:, :HEAD]
        query = pre * jax.nn.sigmoid(pre)
        value = total[:, 2 * HEAD :]
        decayed = query
        result = jnp.sum(query * key, axis=1, keepdims=True) * value
        for back in range(1, STEPS):
            gate_back = gate if back == 1 else pltpu.roll(gate, back - 1, 0)
            decayed = decayed * (
                gate_back if back == 1 else jnp.where(when >= back - 1, gate_back, 1.0)
            )
            weight = jnp.sum(
                jnp.where(when >= back, decayed * pltpu.roll(key, back, 0), 0.0),
                axis=1,
                keepdims=True,
            )
            result = result + weight * pltpu.roll(value, back, 0)
        decayed = decayed * jnp.where(when >= STEPS - 1, pltpu.roll(gate, STEPS - 1, 0), 1.0)
        low = decayed.astype(BF16)
        carried = []
        for pair in range(SEQS // 2):
            rows = low[pair * 8 : pair * 8 + 8]
            one = jnp.dot(rows, base_low[2 * pair, h], preferred_element_type=F32)
            two = jnp.dot(rows, base_low[2 * pair + 1, h], preferred_element_type=F32)
            carried.append(jnp.where(first_seq, one, two))
        result = result + jnp.concatenate(carried, axis=0)
        mean = jnp.sum(result * result, axis=1, keepdims=True) / HEAD
        normed = result * lax.rsqrt(mean + EPSILON) * head_gain_ref[h : h + 1, :]
        normed_all[z, h] = normed.astype(BF16)
        slot = normed_all.at[z, h]
        for i, dz in enumerate((4, 3, 5, 2, 6, 1, 7)):
            normed_copies.append(
                go(remote(slot, slot, normed_sems, h * 7 + i, (at_z(dz), y, c, x)))
            )

    w_forward(0)
    w_complete(0)
    sqz_copies = squares_out()
    for copy in x_copies:
        copy.wait_recv()
    left = jnp.transpose(x_all[...].reshape(G * FEATS, SET))
    multiply(0, left)
    w_forward(1)
    merge(0)
    w_complete(1)
    multiply(1, left)
    w_forward(2)
    w_complete(2)
    multiply(2, left)
    merge(1)
    w_forward(3)
    w_complete(3)
    multiply(3, left)
    rscale = token_scale(sqz_copies)
    recur(0, rscale)
    merge(2)
    merge(3)
    recur(1, rscale)
    w_forward(4)
    recur(2, rscale)
    recur(3, rscale)
    w_complete(4)

    for copy in normed_copies:
        copy.wait_recv()

    product = None
    for h in range(HEADS):
        term = lax.dot_general(
            wo_all[:, :, pl.ds(h * HEAD, HEAD)].reshape(G * FEATS, HEAD),
            normed_all[:, h].reshape(SET, HEAD),
            (((1,), (1,)), ((), ())),
            preferred_element_type=F32,
        )
        product = term if product is None else product + term
    final_send[...] = product.astype(BF16).reshape(G, X, FEATS // X, SET)
    copies = []
    final_recv[x, g] = final_send[g, x]
    for i, (dy, dc, dx) in enumerate(
        [(dy, dc, dx) for dy in (2, 1, 3, 0) for dx in (2, 1, 3, 0) for dc in (0, 1) if dy or dx or dc]
    ):
        py, pc = group_peer(dy, dc)
        px = at_x(dx)
        src, dst = final_send.at[py * C + pc, px], final_recv.at[x, g]
        copies.append(go(remote(src, dst, final_sems, i, (z, py, pc, px))))
    for copy in copies:
        copy.wait_recv()

    rows_out = FEATS // X
    for k in range(G):
        total = final_recv[0, k].astype(F32)
        for m in range(1, X):
            total = total + final_recv[m, k].astype(F32)
        out_ref[k] = total.astype(BF16)

    for copy in started:
        copy.wait_send()


def tail(pieces_ref, base_ref, out_ref, base_hbm, sems):
    stores = []
    for s in range(SEQS):
        store = pltpu.make_async_copy(base_ref.at[s], base_hbm.at[s], sems.at[s])
        store.start()
        stores.append(store)
    rows_out = FEATS // X
    lane_block = lax.broadcasted_iota(jnp.int32, (rows_out, HEAD), 1) // OWN
    for zz in range(Z):
        for half_g in range(2):
            tile = None
            for k in range(4):
                src = pieces_ref[half_g * 4 + k, :, pl.ds((zz // 4) * 128, 128)].astype(F32)
                shift = ((k - zz % 4) * OWN) % 128
                if shift:
                    src = pltpu.roll(src, shift, 1)
                tile = src if tile is None else jnp.where(lane_block == k, src, tile)
            out_ref[:, pl.ds(zz * 256 + half_g * 128, 128)] = tile.astype(BF16)
    for store in stores:
        store.wait()


def fused(*args):
    any_space = pl.BlockSpec(memory_space=pl.ANY)
    vmem = pl.BlockSpec(memory_space=pltpu.VMEM)
    smem = pl.BlockSpec(memory_space=pltpu.SMEM)
    dma = lambda n: pltpu.SemaphoreType.DMA((2, n))
    pieces, base = pl.pallas_call(
        kernel,
        out_shape=(
            pltpu.VMEM((G, FEATS // X, SET), BF16),
            pltpu.VMEM((SEQS, HEADS, HEAD, HEAD), F32),
        ),
        in_specs=[any_space, vmem] + [any_space] * 4 + [vmem, vmem, any_space, vmem, vmem, smem],
        out_specs=(vmem, vmem),
        scratch_shapes=[
            pltpu.VMEM((FEATS, TOKENS), BF16),
            pltpu.VMEM((G, FEATS, SET), BF16),
            pltpu.VMEM((G, FEATS, SET), BF16),
            pltpu.VMEM((G, 1, SET), F32),
            pltpu.VMEM((G, 1, SET), F32),
            pltpu.VMEM((1, SET), F32),
            pltpu.VMEM((Z, 1, SET), F32),
            pltpu.VMEM((HEADS, G, FEATS, WIDE), BF16),
            pltpu.VMEM((G, FEATS, COLS), BF16),
            pltpu.VMEM((SEQS, HEADS, HEAD, HEAD), BF16),
            pltpu.VMEM((HEADS, Z, OWN, WIDE), F32),
            pltpu.VMEM((HEADS, 2, 2, OWN, WIDE), BF16),
            pltpu.VMEM((HEADS, 2, 2, OWN, WIDE), BF16),
            pltpu.VMEM((HEADS, 2, 2, OWN, WIDE), BF16),
            pltpu.VMEM((HEADS, 2, 2, OWN, WIDE), BF16),
            pltpu.VMEM((Z, HEADS, OWN, HEAD), BF16),
            pltpu.VMEM((G, X, FEATS // X, SET), BF16),
            pltpu.VMEM((X, G, FEATS // X, SET), BF16),
            pltpu.SemaphoreType.DMA((15,)),
            dma(G - 1),
            dma(G - 1),
            dma(Z - 1),
            dma((HEADS + 1) * 7),
            dma(HEADS * 4),
            dma(HEADS * 4),
            dma(HEADS * 7),
            dma(G * X - 1),
        ],
        compiler_params=pltpu.CompilerParams(collective_id=0, has_side_effects=True),
    )(*args)
    return pl.pallas_call(
        tail,
        out_shape=(
            jax.ShapeDtypeStruct((FEATS // X, TOKENS), BF16),
            jax.ShapeDtypeStruct((SEQS, HEADS, HEAD, HEAD), F32),
        ),
        in_specs=[vmem, vmem],
        out_specs=(vmem, any_space),
        scratch_shapes=[pltpu.SemaphoreType.DMA((SEQS,))],
        compiler_params=pltpu.CompilerParams(vmem_limit_bytes=8 * 2**20),
    )(pieces, base)


def body(
    inputs,
    norm_gain,
    w_query,
    w_forget,
    w_value,
    lower_bound,
    head_gain,
    w_out,
    prior_state,
    prev_forget,
    prev_values,
    accepted,
):
    mixed, base_state = fused(
        inputs.T,
        norm_gain.reshape(1, FEATS),
        w_query,
        w_forget,
        w_value,
        w_out.T,
        lower_bound.reshape(HEADS, HEAD),
        head_gain.reshape(HEADS, HEAD),
        prior_state,
        prev_forget,
        prev_values,
        accepted,
    )
    return (mixed.T, base_state)


def solution(mesh):
    split = Mesh(mesh.devices.reshape(Z, Y, C, X), KV_TP)
    placed = (
        P(None, KV),
        P(KV),
        P(KV, "tp"),
        P(KV, "tp"),
        P(KV, "tp"),
        P("tp"),
        P("tp"),
        P("tp", KV),
        P(KV, "tp", None, None),
        P(KV, None, "tp"),
        P(KV, None, "tp"),
        P(KV),
    )
    return jax.shard_map(
        body,
        mesh=split,
        in_specs=placed,
        out_specs=(P(None, KV_TP), P(KV, "tp", None, None)),
        check_vma=False,
    )
```

time: 65.5 us -> 54.5 us (0.83)
  Pallas kernels: 60 us -> 53.7 us
  local copies, waits for them, and re-layouts: 4.61 us -> 0 us
    pallas_call x1 -> x2, Pallas kernels: 60 us -> 53.7 us  [the longest x1 51.7 us: fused(): pl.pallas_call(kernel, out_shape=(pltpu.VMEM((G, FEATS // X, SET), BF16),...]
    unnamed x2 -> x0, local copies, waits for them, and re-layouts: 4.61 us -> none
where the time goes in v2:
time: 54.5 us; the launch traced here: 54.4 us
  Pallas kernels  53.7 us (99%)
  between operations  0.64 us (1%)
    pallas_call x1, Pallas kernels, fused(): pl.pallas_call(kernel, out_shape=(pltpu.VMEM((G, FEATS // X, SET), BF16),...  51.7 us
    pallas_call x1, Pallas kernels, fused(): pl.pallas_call(tail, out_shape=(jax.ShapeDtypeStruct((FEATS // X, TOKENS)...  2.01 us

profile of v2, /device:TPU:1, one launch (start us, length us, event | category | flops | bytes accessed | tf_op | source)
XLA Modules:
  0.0 54.4 jit_solution(7714102362274201680)
XLA Ops:
  0.6 51.7 %shard_map.131 = (bf16[8,16,256]{2,1,0:T(8,128)(2,1)S(1)}, f32[8,4,128,128]{3,2,1,0:T(8,128)S(1)}) custom-call(bf16[64,2048]{1,0:T(8,128)(2,1)} %bitcast.6, bf16[1,64]{1,0:T(2,128)(2,1)} %bitcast.10, bf16[64,512]{1,0:T(8,128)(2,1)} %wq_hbm.1, bf16[64,512]{1,0:T(8,128)(2,1)} %wf_hbm.1, bf16[64,512]{1,0:T(8,128)(2,1)} %wv_hbm.1, bf16[64,512]{1,0:T(8,128)(2,1)} %bitcast.7, ...), custom_call_target="tpu_custom_call" | custom-call | tf_op jit(solution)/shard_map/pallas_call | solution.py:437
  52.4 2.0 %shard_map.132 = (bf16[16,2048]{1,0:T(8,128)(2,1)}, f32[8,4,128,128]{3,2,1,0:T(8,128)}) custom-call(bf16[8,16,256]{2,1,0:T(8,128)(2,1)S(1)} %get-tuple-element.6.pieces_ref, f32[8,4,128,128]{3,2,1,0:T(8,128)S(1)} %get-tuple-element.7.base_ref), custom_call_target="tpu_custom_call" | custom-call | tf_op jit(solution)/shard_map/pallas_call | solution.py:476

commit v3 on v2

--- a/solution.py
+++ b/solution.py
@@ -35,22 +35,29 @@
 
 def kernel(
     x_hbm,
-    gain_ref,
+    gain_hbm,
     wq_hbm,
     wf_hbm,
     wv_hbm,
     wo_hbm,
+    floor_hbm,
+    head_gain_hbm,
+    prior_hbm,
+    prev_gate_hbm,
+    prev_value_hbm,
+    accepted_hbm,
+    out_ref,
+    base_ref,
+    gain_ref,
     floor_ref,
     head_gain_ref,
-    prior_hbm,
     prev_gate_ref,
     prev_value_ref,
     accepted_ref,
-    out_ref,
-    base_ref,
     x_raw,
     x_send,
     x_all,
+    left_ref,
     sq_send,
     sq_all,
     sq_mine,
@@ -66,6 +73,7 @@
     normed_all,
     final_send,
     final_recv,
+    relay_sem,
     local_sem,
     x_sems,
     sq_sems,
@@ -98,38 +106,101 @@
         return at_y(dy), (sib if dc else c)
 
     barrier = pltpu.get_barrier_semaphore()
-    peers = [(at_z(dz), y, c, x) for dz in (4, 3, 5, 2, 6, 1, 7)]
+    z_near = [(at_z(1), y, c, x), (at_z(-1), y, c, x)]
+    peers = []
     for dy, dc in group_steps:
         py, pc = group_peer(dy, dc)
         peers.append((z, py, pc, x))
-    for dx in range(1, X):
+    for dx in (2, 1, 3):
         peers.append((z, y, c, at_x(dx)))
-    for peer in peers:
+    for peer in peers + z_near:
         pl.semaphore_signal(barrier, inc=1, device_id=peer, device_id_type=MESH_ID)
 
-    x_load = pltpu.make_async_copy(x_hbm, x_raw, local_sem.at[0])
-    x_load.start()
-    w_loads = []
-    for h in range(HEADS):
-        loads = []
-        for k, src in enumerate((wq_hbm, wf_hbm, wv_hbm)):
-            load = pltpu.make_async_copy(
+    def load(src, dst, index):
+        copy = pltpu.make_async_copy(src, dst, local_sem.at[index])
+        copy.start()
+        return copy
+
+    def load_weights(h):
+        return [
+            load(
                 src.at[:, pl.ds(h * HEAD, HEAD)],
-                w_all.at[h, g, :, pl.ds(k * HEAD, HEAD)],
-                local_sem.at[3 + h * 3 + k],
+                w_all.at[h, 0, 0, :, pl.ds(k * HEAD, HEAD)],
+                3 + h * 3 + k,
             )
-            load.start()
-            loads.append(load)
-        w_loads.append(loads)
-    wo_load = pltpu.make_async_copy(wo_hbm, wo_all.at[g], local_sem.at[1])
-    wo_load.start()
-    w_loads.append([wo_load])
-    prior_load = pltpu.make_async_copy(prior_hbm, base_ref, local_sem.at[2])
-    prior_load.start()
-
+            for k, src in enumerate((wq_hbm, wf_hbm, wv_hbm))
+        ]
+
+    w_loads = [load_weights(0)]
+    x_load = load(x_hbm, x_raw, 0)
+    gain_load = load(gain_hbm, gain_ref, 15)
+    w_loads += [load_weights(h) for h in range(1, HEADS)]
+    base_loads = [
+        load(prior_hbm, base_ref, 2),
+        load(prev_gate_hbm, prev_gate_ref, 18),
+        load(prev_value_hbm, prev_value_ref, 19),
+        load(accepted_hbm, accepted_ref, 20),
+    ]
+    small_loads = [load(floor_hbm, floor_ref, 16), load(head_gain_hbm, head_gain_ref, 17)]
+    w_loads.append([load(wo_hbm, wo_all.at[0, 0], 1)])
+
+    for copy in w_loads[0]:
+        copy.wait()
+    pl.semaphore_wait(barrier, len(peers + z_near))
+
+    def relay_out(k):
+        for peer in z_near:
+            pl.semaphore_signal(relay_sem.at[k], inc=1, device_id=peer, device_id_type=MESH_ID)
+
+    def relay_in(k):
+        pl.semaphore_wait(relay_sem.at[k], 2)
+
+    relay_out(0)
+
+    def remote(src, dst, sems, index, peer):
+        return pltpu.make_async_remote_copy(
+            src_ref=src,
+            dst_ref=dst,
+            send_sem=sems.at[0, index],
+            recv_sem=sems.at[1, index],
+            device_id=peer,
+            device_id_type=MESH_ID,
+        )
+
+    started = []
+
+    def go(copy):
+        copy.start()
+        started.append(copy)
+        return copy
+
+    W = [{} for _ in range(HEADS + 1)]
+
+    def w_slot(j, dy, dc):
+        return w_all.at[j, dy, dc] if j < HEADS else wo_all.at[dy, dc]
+
+    def w_out(j):
+        own = w_slot(j, 0, 0)
+        for i, dy in enumerate((2, 1, 3)):
+            W[j][dy] = go(remote(own, w_slot(j, dy, 0), w_sems, j * 7 + i, (z, at_y(dy), c, x)))
+        W[j]["sib", 0] = go(remote(own, w_slot(j, 0, 1), w_sems, j * 7 + 3, (z, y, sib, x)))
+
+    def w_forward(j):
+        for i, dy in enumerate((1, 3, 2)):
+            W[j][dy].wait_recv()
+            src, dst = w_slot(j, dy, 0), w_slot(j, dy, 1)
+            W[j]["sib", dy] = go(remote(src, dst, w_sems, j * 7 + 4 + i, (z, y, sib, x)))
+
+    def w_complete(j):
+        for dy in (0, 1, 3, 2):
+            W[j]["sib", dy].wait_recv()
+
+    w_out(0)
+
+    x_load.wait()
+    gain_load.wait()
     gain_col = jnp.transpose(jnp.broadcast_to(gain_ref[...].astype(F32), (HEAD, FEATS)))
     lane_block = lax.broadcasted_iota(jnp.int32, (FEATS, HEAD), 1) // OWN
-    x_load.wait()
     for peer in range(G):
         for half in range(2):
             tile = None
@@ -143,63 +214,22 @@
             lanes = pl.ds(half * 128, 128)
             sq_send[peer, :, lanes] = jnp.sum(tile * tile, axis=0, keepdims=True)
             x_send[peer, :, lanes] = (tile * gain_col).astype(BF16)
-
-    pl.semaphore_wait(barrier, len(peers))
-
-    def remote(src, dst, sems, index, peer):
-        return pltpu.make_async_remote_copy(
-            src_ref=src,
-            dst_ref=dst,
-            send_sem=sems.at[0, index],
-            recv_sem=sems.at[1, index],
-            device_id=peer,
-            device_id_type=MESH_ID,
-        )
-
-    started = []
-
-    def go(copy):
-        copy.start()
-        started.append(copy)
-        return copy
-
-    W = [{} for _ in range(HEADS + 1)]
-
-    def w_slot(j, member):
-        return w_all.at[j, member] if j < HEADS else wo_all.at[member]
-
-    def w_out(j):
-        for load in w_loads[j]:
-            load.wait()
-        own = w_slot(j, g)
-        for i, dy in enumerate((2, 1, 3)):
-            W[j][dy] = go(remote(own, own, w_sems, j * 7 + i, (z, at_y(dy), c, x)))
-        W[j]["sib", 0] = go(remote(own, own, w_sems, j * 7 + 3, (z, y, sib, x)))
-
-    def w_forward(j):
-        for i, dy in enumerate((1, 3, 2)):
-            W[j][dy].wait_recv()
-            block = w_slot(j, at_y(-dy) * C + c)
-            W[j]["sib", dy] = go(remote(block, block, w_sems, j * 7 + 4 + i, (z, y, sib, x)))
-
-    def w_complete(j):
-        for dy in (0, 1, 3, 2):
-            W[j]["sib", dy].wait_recv()
-
-    w_out(0)
-    x_copies, sq_copies = [], []
+    X_in = {}
+    sq_copies = []
     for i, (dy, dc) in enumerate(group_steps):
         py, pc = group_peer(dy, dc)
         pg = py * C + pc
         peer = (z, py, pc, x)
-        x_copies.append(go(remote(x_send.at[pg], x_all.at[g], x_sems, i, peer)))
-        sq_copies.append(go(remote(sq_send.at[pg], sq_all.at[g], sq_sems, i, peer)))
+        X_in[dy, dc] = go(remote(x_send.at[pg], x_all.at[dy, dc], x_sems, i, peer))
+        sq_copies.append(go(remote(sq_send.at[pg], sq_all.at[i], sq_sems, i, peer)))
     for j in range(1, HEADS + 1):
+        for copy in w_loads[j]:
+            copy.wait()
         w_out(j)
-    x_all[g] = x_send[g]
-    sq_all[g] = sq_send[g]
-
-    prior_load.wait()
+    x_all[0, 0] = x_send[g]
+
+    for copy in base_loads:
+        copy.wait()
     position = lax.broadcasted_iota(jnp.int32, (STEPS, COLS), 0)
     decays, keys_old, values_old = [], [], []
     for s in range(SEQS):
@@ -234,8 +264,8 @@
     def squares_out():
         for copy in sq_copies:
             copy.wait_recv()
-        total = sq_all[0]
-        for k in range(1, G):
+        total = sq_send[g]
+        for k in range(G - 1):
             total = total + sq_all[k]
         sq_mine[...] = total
         copies = []
@@ -262,8 +292,18 @@
 
     first, second = {}, {}
 
-    def multiply(j, left):
-        product = jnp.dot(left, w_all[j].reshape(G * FEATS, WIDE), preferred_element_type=F32)
+    def inputs_in():
+        for dy in (0, 1, 3, 2):
+            for dc in range(C):
+                if dy or dc:
+                    X_in[dy, dc].wait_recv()
+            block = x_all[dy].reshape(C * FEATS, SET)
+            left_ref[:, pl.ds(dy * C * FEATS, C * FEATS)] = jnp.transpose(block)
+
+    def multiply(j):
+        product = jnp.dot(
+            left_ref[...], w_all[j].reshape(G * FEATS, WIDE), preferred_element_type=F32
+        )
         part[j] = product.reshape(Z, OWN, WIDE)
         for way, sign in ((UP, 1), (DOWN, -1)):
             for m, (far, near) in enumerate(MERGES[HOPS[j][way]]):
@@ -297,7 +337,7 @@
     row = lax.broadcasted_iota(jnp.int32, (OWN, HEAD), 0)
     when = lax.rem(row, STEPS)
     first_seq = lax.broadcasted_iota(jnp.int32, (8, HEAD), 0) < STEPS
-    normed_copies = []
+    normed_copies = [[] for _ in range(HEADS)]
 
     def recur(h, rscale):
         total = part[h, z]
@@ -339,59 +379,63 @@
         normed_all[z, h] = normed.astype(BF16)
         slot = normed_all.at[z, h]
         for i, dz in enumerate((4, 3, 5, 2, 6, 1, 7)):
-            normed_copies.append(
+            normed_copies[h].append(
                 go(remote(slot, slot, normed_sems, h * 7 + i, (at_z(dz), y, c, x)))
             )
 
+    relay_in(0)
+    relay_out(1)
     w_forward(0)
+    relay_in(1)
+    relay_out(2)
     w_complete(0)
+    inputs_in()
+    multiply(0)
+    relay_in(2)
     sqz_copies = squares_out()
-    for copy in x_copies:
-        copy.wait_recv()
-    left = jnp.transpose(x_all[...].reshape(G * FEATS, SET))
-    multiply(0, left)
+    for copy in small_loads:
+        copy.wait()
     w_forward(1)
     merge(0)
     w_complete(1)
-    multiply(1, left)
+    multiply(1)
     w_forward(2)
     w_complete(2)
-    multiply(2, left)
-    merge(1)
+    multiply(2)
     w_forward(3)
     w_complete(3)
-    multiply(3, left)
+    multiply(3)
+    merge(1)
     rscale = token_scale(sqz_copies)
-    recur(0, rscale)
     merge(2)
     merge(3)
+    recur(0, rscale)
     recur(1, rscale)
     w_forward(4)
     recur(2, rscale)
     recur(3, rscale)
     w_complete(4)
 
-    for copy in normed_copies:
-        copy.wait_recv()
-
     product = None
     for h in range(HEADS):
+        for copy in normed_copies[h]:
+            copy.wait_recv()
         term = lax.dot_general(
-            wo_all[:, :, pl.ds(h * HEAD, HEAD)].reshape(G * FEATS, HEAD),
+            wo_all[:, :, :, pl.ds(h * HEAD, HEAD)].reshape(G * FEATS, HEAD),
             normed_all[:, h].reshape(SET, HEAD),
             (((1,), (1,)), ((), ())),
             preferred_element_type=F32,
         )
         product = term if product is None else product + term
-    final_send[...] = product.astype(BF16).reshape(G, X, FEATS // X, SET)
+    final_send[...] = product.astype(BF16).reshape(Y, C, X, FEATS // X, SET)
     copies = []
-    final_recv[x, g] = final_send[g, x]
+    final_recv[x, g] = final_send[0, 0, x]
     for i, (dy, dc, dx) in enumerate(
         [(dy, dc, dx) for dy in (2, 1, 3, 0) for dx in (2, 1, 3, 0) for dc in (0, 1) if dy or dx or dc]
     ):
-        py, pc = group_peer(dy, dc)
+        py, pc = at_y(-dy), (sib if dc else c)
         px = at_x(dx)
-        src, dst = final_send.at[py * C + pc, px], final_recv.at[x, g]
+        src, dst = final_send.at[dy, dc, px], final_recv.at[x, g]
         copies.append(go(remote(src, dst, final_sems, i, (z, py, pc, px))))
     for copy in copies:
         copy.wait_recv()
@@ -432,7 +476,6 @@
 def fused(*args):
     any_space = pl.BlockSpec(memory_space=pl.ANY)
     vmem = pl.BlockSpec(memory_space=pltpu.VMEM)
-    smem = pl.BlockSpec(memory_space=pltpu.SMEM)
     dma = lambda n: pltpu.SemaphoreType.DMA((2, n))
     pieces, base = pl.pallas_call(
         kernel,
@@ -440,18 +483,25 @@
             pltpu.VMEM((G, FEATS // X, SET), BF16),
             pltpu.VMEM((SEQS, HEADS, HEAD, HEAD), F32),
         ),
-        in_specs=[any_space, vmem] + [any_space] * 4 + [vmem, vmem, any_space, vmem, vmem, smem],
+        in_specs=[any_space] * 12,
         out_specs=(vmem, vmem),
         scratch_shapes=[
+            pltpu.VMEM((1, FEATS), BF16),
+            pltpu.VMEM((HEADS, HEAD), F32),
+            pltpu.VMEM((HEADS, HEAD), F32),
+            pltpu.VMEM((SEQS, STEPS, COLS), F32),
+            pltpu.VMEM((SEQS, STEPS, COLS), BF16),
+            pltpu.SMEM((SEQS,), jnp.int32),
             pltpu.VMEM((FEATS, TOKENS), BF16),
             pltpu.VMEM((G, FEATS, SET), BF16),
-            pltpu.VMEM((G, FEATS, SET), BF16),
+            pltpu.VMEM((Y, C, FEATS, SET), BF16),
+            pltpu.VMEM((SET, G * FEATS), BF16),
             pltpu.VMEM((G, 1, SET), F32),
-            pltpu.VMEM((G, 1, SET), F32),
+            pltpu.VMEM((G - 1, 1, SET), F32),
             pltpu.VMEM((1, SET), F32),
             pltpu.VMEM((Z, 1, SET), F32),
-            pltpu.VMEM((HEADS, G, FEATS, WIDE), BF16),
-            pltpu.VMEM((G, FEATS, COLS), BF16),
+            pltpu.VMEM((HEADS, Y, C, FEATS, WIDE), BF16),
+            pltpu.VMEM((Y, C, FEATS, COLS), BF16),
             pltpu.VMEM((SEQS, HEADS, HEAD, HEAD), BF16),
             pltpu.VMEM((HEADS, Z, OWN, WIDE), F32),
             pltpu.VMEM((HEADS, 2, 2, OWN, WIDE), BF16),
@@ -459,9 +509,10 @@
             pltpu.VMEM((HEADS, 2, 2, OWN, WIDE), BF16),
             pltpu.VMEM((HEADS, 2, 2, OWN, WIDE), BF16),
             pltpu.VMEM((Z, HEADS, OWN, HEAD), BF16),
-            pltpu.VMEM((G, X, FEATS // X, SET), BF16),
+            pltpu.VMEM((Y, C, X, FEATS // X, SET), BF16),
             pltpu.VMEM((X, G, FEATS // X, SET), BF16),
-            pltpu.SemaphoreType.DMA((15,)),
+            pltpu.SemaphoreType.REGULAR((3,)),
+            pltpu.SemaphoreType.DMA((21,)),
             dma(G - 1),
             dma(G - 1),
             dma(Z - 1),

time: 54.5 us -> 51.6 us (0.947)
  Pallas kernels: 53.7 us -> 50.9 us
    pallas_call x1, Pallas kernels: 51.7 us -> 48.9 us  [fused(): pl.pallas_call(kernel, out_shape=(pltpu.VMEM((G, FEATS // X, SET), BF16),...]
where the time goes in v3:
time: 51.6 us; the launch traced here: 51.5 us
  Pallas kernels  50.9 us (99%)
  between operations  0.64 us (1%)
    pallas_call x1, Pallas kernels, fused(): pl.pallas_call(kernel, out_shape=(pltpu.VMEM((G, FEATS // X, SET), BF16),...  48.9 us
    pallas_call x1, Pallas kernels, fused(): pl.pallas_call(tail, out_shape=(jax.ShapeDtypeStruct((FEATS // X, TOKENS)...  2.01 us

profile of v3, /device:TPU:1, one launch (start us, length us, event | category | flops | bytes accessed | tf_op | source)
XLA Modules:
  0.0 51.5 jit_solution(10097246170719611525)
XLA Ops:
  0.6 48.9 %shard_map.131 = (bf16[8,16,256]{2,1,0:T(8,128)(2,1)S(1)}, f32[8,4,128,128]{3,2,1,0:T(8,128)S(1)}) custom-call(bf16[64,2048]{1,0:T(8,128)(2,1)} %bitcast.6, bf16[1,64]{1,0:T(2,128)(2,1)} %bitcast.10, bf16[64,512]{1,0:T(8,128)(2,1)} %wq_hbm.1, bf16[64,512]{1,0:T(8,128)(2,1)} %wf_hbm.1, bf16[64,512]{1,0:T(8,128)(2,1)} %wv_hbm.1, bf16[64,512]{1,0:T(8,128)(2,1)} %bitcast.7, ...), custom_call_target="tpu_custom_call" | custom-call | tf_op jit(solution)/shard_map/pallas_call | solution.py:480
  49.5 2.0 %shard_map.132 = (bf16[16,2048]{1,0:T(8,128)(2,1)}, f32[8,4,128,128]{3,2,1,0:T(8,128)}) custom-call(bf16[8,16,256]{2,1,0:T(8,128)(2,1)S(1)} %get-tuple-element.6.pieces_ref, f32[8,4,128,128]{3,2,1,0:T(8,128)S(1)} %get-tuple-element.7.base_ref), custom_call_target="tpu_custom_call" | custom-call | tf_op jit(solution)/shard_map/pallas_call | solution.py:527

commit v4 on v3

--- a/solution.py
+++ b/solution.py
@@ -29,8 +29,12 @@
 STEPS = 4
 UP, DOWN = 0, 1
 WIDE = 3 * HEAD
+CHUNKS = ((0, 384), (384, 384), (768, 384), (1152, 384))
 HOPS = ((4, 3), (3, 4), (4, 3), (3, 4))
+SLOT = (0, 1, 3, 2)
 MERGES = {4: ((4, 3), (2, 1)), 3: ((3, 2), (None, 1))}
+KINDS = 10
+ARRIVALS = 36
 
 
 def kernel(
@@ -58,6 +62,8 @@
     x_send,
     x_all,
     left_ref,
+    half_send,
+    half_recv,
     sq_send,
     sq_all,
     sq_mine,
@@ -75,14 +81,8 @@
     final_recv,
     relay_sem,
     local_sem,
-    x_sems,
-    sq_sems,
-    sqz_sems,
-    w_sems,
-    first_sems,
-    second_sems,
-    normed_sems,
-    final_sems,
+    send_sems,
+    recv_sems,
 ):
     z = lax.axis_index("kv_0")
     y = lax.axis_index("kv_1")
@@ -121,81 +121,26 @@
         copy.start()
         return copy
 
-    def load_weights(h):
-        return [
-            load(
-                src.at[:, pl.ds(h * HEAD, HEAD)],
-                w_all.at[h, 0, 0, :, pl.ds(k * HEAD, HEAD)],
-                3 + h * 3 + k,
-            )
-            for k, src in enumerate((wq_hbm, wf_hbm, wv_hbm))
-        ]
+    def load_weights(j):
+        start, width = CHUNKS[j]
+        for k in range(start // HEAD, (start + width) // HEAD):
+            src = (wq_hbm, wf_hbm, wv_hbm)[k % 3].at[:, pl.ds(k // 3 * HEAD, HEAD)]
+            load(src, w_all.at[0, :, pl.ds(k * HEAD, HEAD)], j)
+        own = w_all.at[0, :, pl.ds(start, width)]
+        return [pltpu.make_async_copy(own, own, local_sem.at[j])]
 
     w_loads = [load_weights(0)]
-    x_load = load(x_hbm, x_raw, 0)
-    gain_load = load(gain_hbm, gain_ref, 15)
-    w_loads += [load_weights(h) for h in range(1, HEADS)]
+    x_load = load(x_hbm, x_raw, 4)
+    gain_load = load(gain_hbm, gain_ref, 5)
+    w_loads += [load_weights(j) for j in range(1, len(CHUNKS))]
     base_loads = [
-        load(prior_hbm, base_ref, 2),
-        load(prev_gate_hbm, prev_gate_ref, 18),
-        load(prev_value_hbm, prev_value_ref, 19),
-        load(accepted_hbm, accepted_ref, 20),
+        load(prior_hbm, base_ref, 6),
+        load(prev_gate_hbm, prev_gate_ref, 7),
+        load(prev_value_hbm, prev_value_ref, 8),
+        load(accepted_hbm, accepted_ref, 9),
     ]
-    small_loads = [load(floor_hbm, floor_ref, 16), load(head_gain_hbm, head_gain_ref, 17)]
-    w_loads.append([load(wo_hbm, wo_all.at[0, 0], 1)])
-
-    for copy in w_loads[0]:
-        copy.wait()
-    pl.semaphore_wait(barrier, len(peers + z_near))
-
-    def relay_out(k):
-        for peer in z_near:
-            pl.semaphore_signal(relay_sem.at[k], inc=1, device_id=peer, device_id_type=MESH_ID)
-
-    def relay_in(k):
-        pl.semaphore_wait(relay_sem.at[k], 2)
-
-    relay_out(0)
-
-    def remote(src, dst, sems, index, peer):
-        return pltpu.make_async_remote_copy(
-            src_ref=src,
-            dst_ref=dst,
-            send_sem=sems.at[0, index],
-            recv_sem=sems.at[1, index],
-            device_id=peer,
-            device_id_type=MESH_ID,
-        )
-
-    started = []
-
-    def go(copy):
-        copy.start()
-        started.append(copy)
-        return copy
-
-    W = [{} for _ in range(HEADS + 1)]
-
-    def w_slot(j, dy, dc):
-        return w_all.at[j, dy, dc] if j < HEADS else wo_all.at[dy, dc]
-
-    def w_out(j):
-        own = w_slot(j, 0, 0)
-        for i, dy in enumerate((2, 1, 3)):
-            W[j][dy] = go(remote(own, w_slot(j, dy, 0), w_sems, j * 7 + i, (z, at_y(dy), c, x)))
-        W[j]["sib", 0] = go(remote(own, w_slot(j, 0, 1), w_sems, j * 7 + 3, (z, y, sib, x)))
-
-    def w_forward(j):
-        for i, dy in enumerate((1, 3, 2)):
-            W[j][dy].wait_recv()
-            src, dst = w_slot(j, dy, 0), w_slot(j, dy, 1)
-            W[j]["sib", dy] = go(remote(src, dst, w_sems, j * 7 + 4 + i, (z, y, sib, x)))
-
-    def w_complete(j):
-        for dy in (0, 1, 3, 2):
-            W[j]["sib", dy].wait_recv()
-
-    w_out(0)
+    small_loads = [load(floor_hbm, floor_ref, 10), load(head_gain_hbm, head_gain_ref, 11)]
+    w_loads.append([load(wo_hbm, wo_all.at[0], 12)])
 
     x_load.wait()
     gain_load.wait()
@@ -214,19 +159,65 @@
             lanes = pl.ds(half * 128, 128)
             sq_send[peer, :, lanes] = jnp.sum(tile * tile, axis=0, keepdims=True)
             x_send[peer, :, lanes] = (tile * gain_col).astype(BF16)
-    X_in = {}
-    sq_copies = []
+
+    pl.semaphore_wait(barrier, len(peers + z_near))
+
+    def relay_out(k):
+        for peer in z_near:
+            pl.semaphore_signal(relay_sem.at[k], inc=1, device_id=peer, device_id_type=MESH_ID)
+
+    def relay_in(k):
+        pl.semaphore_wait(relay_sem.at[k], 2)
+
+    relay_out(0)
+
+    kinds, arrivals = {}, {}
+
+    def go(src, dst, kind, arrival, peer):
+        copy = pltpu.make_async_remote_copy(
+            src_ref=src,
+            dst_ref=dst,
+            send_sem=send_sems.at[kinds.setdefault(kind, len(kinds))],
+            recv_sem=recv_sems.at[arrivals.setdefault((kind, arrival), len(arrivals))],
+            device_id=peer,
+            device_id_type=MESH_ID,
+        )
+        copy.start()
+        return copy
+
+    def await_bytes(ref, kind, arrival):
+        sem = recv_sems.at[arrivals[kind, arrival]]
+        pltpu.make_async_copy(ref, ref, sem).wait()
+
+    for dy in (2, 1, 3):
+        py = at_y(dy)
+        src = x_send.at[pl.ds(py * C, C)]
+        go(src, x_all.at[SLOT[dy]], "x", dy, (z, py, c, x))
+    x_all[0] = x_send[pl.ds(y * C, C)]
+
     for i, (dy, dc) in enumerate(group_steps):
         py, pc = group_peer(dy, dc)
-        pg = py * C + pc
-        peer = (z, py, pc, x)
-        X_in[dy, dc] = go(remote(x_send.at[pg], x_all.at[dy, dc], x_sems, i, peer))
-        sq_copies.append(go(remote(sq_send.at[pg], sq_all.at[i], sq_sems, i, peer)))
-    for j in range(1, HEADS + 1):
+        go(sq_send.at[py * C + pc], sq_all.at[i], "sq", 0, (z, py, pc, x))
+
+    for j, (start, width) in enumerate(CHUNKS):
         for copy in w_loads[j]:
             copy.wait()
-        w_out(j)
-    x_all[0, 0] = x_send[g]
+        cols = pl.ds(start, width)
+        for dy in (2, 1, 3):
+            dst = w_all.at[SLOT[dy], :, cols]
+            go(w_all.at[0, :, cols], dst, "w", j, (z, at_y(dy), c, x))
+    w_loads[-1][0].wait()
+    for dy in (2, 1, 3):
+        go(wo_all.at[0], wo_all.at[SLOT[dy] * C], "wo", 0, (z, at_y(dy), c, x))
+    go(wo_all.at[0], wo_all.at[1], "wo", 1, (z, y, sib, x))
+
+    def out_weights_across():
+        await_bytes(wo_all.at[pl.ds(0, Y - 1)], "wo", 0)
+        for k in range(1, Y):
+            go(wo_all.at[k * C], wo_all.at[k * C + 1], "wo", 1, (z, y, sib, x))
+
+    def out_weights_in():
+        await_bytes(wo_all.at[pl.ds(0, Y)], "wo", 1)
 
     for copy in base_loads:
         copy.wait()
@@ -262,22 +253,17 @@
             base_low[s, h] = new.astype(BF16)
 
     def squares_out():
-        for copy in sq_copies:
-            copy.wait_recv()
+        await_bytes(sq_all, "sq", 0)
         total = sq_send[g]
         for k in range(G - 1):
             total = total + sq_all[k]
         sq_mine[...] = total
-        copies = []
         for dz in range(1, Z):
-            peer = (at_z(dz), y, c, x)
-            copies.append(go(remote(sq_mine, sq_z.at[z], sqz_sems, dz - 1, peer)))
+            go(sq_mine, sq_z.at[z], "sqz", 0, (at_z(dz), y, c, x))
         sq_z[z] = total
-        return copies
-
-    def token_scale(copies):
-        for copy in copies:
-            copy.wait_recv()
+
+    def token_scale():
+        await_bytes(sq_z.at[pl.ds(0, Z - 1)], "sqz", 0)
         squares = sq_z[0]
         for k in range(1, Z):
             squares = squares + sq_z[k]
@@ -290,61 +276,69 @@
         )
         return lax.rsqrt(own_squares / D + EPSILON)
 
-    first, second = {}, {}
-
-    def inputs_in():
-        for dy in (0, 1, 3, 2):
-            for dc in range(C):
-                if dy or dc:
-                    X_in[dy, dc].wait_recv()
-            block = x_all[dy].reshape(C * FEATS, SET)
-            left_ref[:, pl.ds(dy * C * FEATS, C * FEATS)] = jnp.transpose(block)
+    def inputs_in(pair):
+        for dy in ((1,), (3, 2))[pair]:
+            await_bytes(x_all.at[SLOT[dy]], "x", dy)
+        for k in range(C):
+            block = jnp.concatenate((x_all[2 * pair, k], x_all[2 * pair + 1, k]), axis=0)
+            left_ref[k, :, pl.ds(pair * HEAD, HEAD)] = jnp.transpose(block)
 
     def multiply(j):
-        product = jnp.dot(
-            left_ref[...], w_all[j].reshape(G * FEATS, WIDE), preferred_element_type=F32
-        )
-        part[j] = product.reshape(Z, OWN, WIDE)
-        for way, sign in ((UP, 1), (DOWN, -1)):
+        start, width = CHUNKS[j]
+        cols = pl.ds(start, width)
+        await_bytes(w_all.at[pl.ds(1, Y - 1), :, cols], "w", j)
+        right = w_all[:, :, cols].reshape(Y * FEATS, width)
+        other = jnp.dot(left_ref[sib], right, preferred_element_type=F32)
+        half_send[:, :, cols] = other.astype(BF16).reshape(Z, OWN, width)
+        go(half_send.at[:, :, cols], half_recv.at[:, :, cols], "half", j, (z, y, sib, x))
+        own = jnp.dot(left_ref[c], right, preferred_element_type=F32)
+        part[:, :, cols] = own.reshape(Z, OWN, width)
+
+    def to_neighbour(j, way, m, value, to):
+        cols = pl.ds(*CHUNKS[j])
+        first_send[way * 2 + m, :, cols] = value.astype(BF16)
+        src, dst = first_send.at[way * 2 + m, :, cols], first_recv.at[way * 2 + m, :, cols]
+        go(src, dst, "first", (j, way, m), (to, y, c, x))
+
+    def to_owner(j, way, m, value, to):
+        cols = pl.ds(*CHUNKS[j])
+        second_send[way * 2 + m, :, cols] = value.astype(BF16)
+        src, dst = second_send.at[way * 2 + m, :, cols], second_recv.at[way * 2 + m, :, cols]
+        go(src, dst, "second", j, (to, y, c, x))
+
+    WAYS = ((UP, 1), (DOWN, -1))
+
+    def distribute(j):
+        cols = pl.ds(*CHUNKS[j])
+        await_bytes(half_recv.at[:, :, cols], "half", j)
+        part[:, :, cols] = part[:, :, cols] + half_recv[:, :, cols].astype(F32)
+        for way, sign in WAYS:
             for m, (far, near) in enumerate(MERGES[HOPS[j][way]]):
-                index = (j * 2 + way) * 2 + m
                 if far is None:
-                    second_send[j, way, m] = part[j, at_z(sign * near)].astype(BF16)
-                    src, dst, sems = second_send.at[j, way, m], second_recv.at[j, way, m], second_sems
-                    second[j, way, m] = go(
-                        remote(src, dst, sems, index, (at_z(sign * near), y, c, x))
-                    )
+                    to_owner(j, way, m, part[at_z(sign * near), :, cols], at_z(sign * near))
                 else:
-                    first_send[j, way, m] = part[j, at_z(sign * far)].astype(BF16)
-                    src, dst, sems = first_send.at[j, way, m], first_recv.at[j, way, m], first_sems
-                    first[j, way, m] = go(remote(src, dst, sems, index, (at_z(sign), y, c, x)))
+                    to_neighbour(j, way, m, part[at_z(sign * far), :, cols], at_z(sign))
 
     def merge(j):
+        cols = pl.ds(*CHUNKS[j])
         for m in range(2):
-            for way, sign in ((UP, 1), (DOWN, -1)):
+            for way, sign in WAYS:
                 far, near = MERGES[HOPS[j][way]][m]
-                if far is None:
-                    continue
-                first[j, way, m].wait_recv()
-                value = part[j, at_z(sign * near)] + first_recv[j, way, m].astype(F32)
-                second_send[j, way, m] = value.astype(BF16)
-                src, dst = second_send.at[j, way, m], second_recv.at[j, way, m]
-                index = (j * 2 + way) * 2 + m
-                second[j, way, m] = go(
-                    remote(src, dst, second_sems, index, (at_z(sign * near), y, c, x))
-                )
+                if far is not None:
+                    await_bytes(first_recv.at[way * 2 + m, :, cols], "first", (j, way, m))
+                    value = part[at_z(sign * near), :, cols]
+                    value = value + first_recv[way * 2 + m, :, cols].astype(F32)
+                    to_owner(j, way, m, value, at_z(sign * near))
 
     row = lax.broadcasted_iota(jnp.int32, (OWN, HEAD), 0)
     when = lax.rem(row, STEPS)
     first_seq = lax.broadcasted_iota(jnp.int32, (8, HEAD), 0) < STEPS
-    normed_copies = [[] for _ in range(HEADS)]
-
     def recur(h, rscale):
-        total = part[h, z]
-        for way in (UP, DOWN):
-            for m in range(2):
-                second[h, way, m].wait_recv()
-                total = total + second_recv[h, way, m].astype(F32)
+        cols = pl.ds(*CHUNKS[h])
+        await_bytes(second_recv.at[:, :, cols], "second", h)
+        total = part[z, :, cols]
+        for k in range(4):
+            total = total + second_recv[k, :, cols].astype(F32)
         total = total * rscale
         floor = floor_ref[h : h + 1, :]
         gate = floor + (1.0 - floor) * jax.nn.sigmoid(total[:, HEAD : 2 * HEAD])
@@ -378,77 +372,80 @@
         normed = result * lax.rsqrt(mean + EPSILON) * head_gain_ref[h : h + 1, :]
         normed_all[z, h] = normed.astype(BF16)
         slot = normed_all.at[z, h]
-        for i, dz in enumerate((4, 3, 5, 2, 6, 1, 7)):
-            normed_copies[h].append(
-                go(remote(slot, slot, normed_sems, h * 7 + i, (at_z(dz), y, c, x)))
-            )
+        for dz in (4, 3, 5, 2, 6, 1, 7):
+            go(slot, slot, "normed", h, (at_z(dz), y, c, x))
 
     relay_in(0)
     relay_out(1)
-    w_forward(0)
+    inputs_in(0)
     relay_in(1)
     relay_out(2)
-    w_complete(0)
-    inputs_in()
+    inputs_in(1)
     multiply(0)
+    distribute(0)
+    multiply(1)
+    distribute(1)
+    multiply(2)
+    merge(0)
+    distribute(2)
     relay_in(2)
-    sqz_copies = squares_out()
+    squares_out()
+    multiply(3)
+    distribute(3)
+    merge(1)
+    merge(2)
+    merge(3)
     for copy in small_loads:
         copy.wait()
-    w_forward(1)
-    merge(0)
-    w_complete(1)
-    multiply(1)
-    w_forward(2)
-    w_complete(2)
-    multiply(2)
-    w_forward(3)
-    w_complete(3)
-    multiply(3)
-    merge(1)
-    rscale = token_scale(sqz_copies)
-    merge(2)
-    merge(3)
+    rscale = token_scale()
     recur(0, rscale)
     recur(1, rscale)
-    w_forward(4)
+    out_weights_across()
     recur(2, rscale)
     recur(3, rscale)
-    w_complete(4)
+    out_weights_in()
 
     product = None
     for h in range(HEADS):
-        for copy in normed_copies[h]:
-            copy.wait_recv()
+        await_bytes(normed_all.at[pl.ds(0, Z - 1), h], "normed", h)
         term = lax.dot_general(
-            wo_all[:, :, :, pl.ds(h * HEAD, HEAD)].reshape(G * FEATS, HEAD),
+            wo_all[:, :, pl.ds(h * HEAD, HEAD)].reshape(G * FEATS, HEAD),
             normed_all[:, h].reshape(SET, HEAD),
             (((1,), (1,)), ((), ())),
             preferred_element_type=F32,
         )
         product = term if product is None else product + term
     final_send[...] = product.astype(BF16).reshape(Y, C, X, FEATS // X, SET)
-    copies = []
-    final_recv[x, g] = final_send[0, 0, x]
-    for i, (dy, dc, dx) in enumerate(
-        [(dy, dc, dx) for dy in (2, 1, 3, 0) for dx in (2, 1, 3, 0) for dc in (0, 1) if dy or dx or dc]
-    ):
-        py, pc = at_y(-dy), (sib if dc else c)
-        px = at_x(dx)
-        src, dst = final_send.at[dy, dc, px], final_recv.at[x, g]
-        copies.append(go(remote(src, dst, final_sems, i, (z, py, pc, px))))
-    for copy in copies:
-        copy.wait_recv()
+    final_recv[x * G + g] = final_send[0, 0, x]
+    for dy, dx, dc in [(dy, dx, dc) for dy in (2, 1, 3, 0) for dx in (2, 1, 3, 0) for dc in (0, 1)]:
+        if dy or dx or dc:
+            peer = (z, at_y(-dy), sib if dc else c, at_x(dx))
+            src, dst = final_send.at[SLOT[dy], dc, peer[3]], final_recv.at[x * G + g]
+            go(src, dst, "final", 0, peer)
+    await_bytes(final_recv.at[pl.ds(0, X * G - 1)], "final", 0)
 
     rows_out = FEATS // X
     for k in range(G):
-        total = final_recv[0, k].astype(F32)
+        total = final_recv[k].astype(F32)
         for m in range(1, X):
-            total = total + final_recv[m, k].astype(F32)
+            total = total + final_recv[m * G + k].astype(F32)
         out_ref[k] = total.astype(BF16)
 
-    for copy in started:
-        copy.wait_send()
+    sent = {
+        "x": x_all.at[pl.ds(1, Y - 1)],
+        "w": w_all.at[pl.ds(1, Y - 1)],
+        "sq": sq_all,
+        "wo": wo_all.at[pl.ds(0, G - 1)],
+        "sqz": sq_z.at[pl.ds(0, Z - 1)],
+        "half": half_recv,
+        "first": first_recv.at[pl.ds(0, 3)],
+        "second": second_recv,
+        "normed": normed_all.at[pl.ds(0, Z - 1)],
+        "final": final_recv.at[pl.ds(0, X * G - 1)],
+    }
+    for kind, ref in sent.items():
+        pltpu.make_async_copy(ref, ref, send_sems.at[kinds[kind]]).wait()
+    assert len(kinds) == KINDS and len(arrivals) == ARRIVALS
 
 
 def tail(pieces_ref, base_ref, out_ref, base_hbm, sems):
@@ -476,7 +473,6 @@
 def fused(*args):
     any_space = pl.BlockSpec(memory_space=pl.ANY)
     vmem = pl.BlockSpec(memory_space=pltpu.VMEM)
-    dma = lambda n: pltpu.SemaphoreType.DMA((2, n))
     pieces, base = pl.pallas_call(
         kernel,
         out_shape=(
@@ -495,32 +491,28 @@
             pltpu.VMEM((FEATS, TOKENS), BF16),
             pltpu.VMEM((G, FEATS, SET), BF16),
             pltpu.VMEM((Y, C, FEATS, SET), BF16),
-            pltpu.VMEM((SET, G * FEATS), BF16),
+            pltpu.VMEM((C, SET, Y * FEATS), BF16),
+            pltpu.VMEM((Z, OWN, HEADS * WIDE), BF16),
+            pltpu.VMEM((Z, OWN, HEADS * WIDE), BF16),
             pltpu.VMEM((G, 1, SET), F32),
             pltpu.VMEM((G - 1, 1, SET), F32),
             pltpu.VMEM((1, SET), F32),
             pltpu.VMEM((Z, 1, SET), F32),
-            pltpu.VMEM((HEADS, Y, C, FEATS, WIDE), BF16),
-            pltpu.VMEM((Y, C, FEATS, COLS), BF16),
+            pltpu.VMEM((Y, FEATS, HEADS * WIDE), BF16),
+            pltpu.VMEM((G, FEATS, COLS), BF16),
             pltpu.VMEM((SEQS, HEADS, HEAD, HEAD), BF16),
-            pltpu.VMEM((HEADS, Z, OWN, WIDE), F32),
-            pltpu.VMEM((HEADS, 2, 2, OWN, WIDE), BF16),
-            pltpu.VMEM((HEADS, 2, 2, OWN, WIDE), BF16),
-            pltpu.VMEM((HEADS, 2, 2, OWN, WIDE), BF16),
-            pltpu.VMEM((HEADS, 2, 2, OWN, WIDE), BF16),
+            pltpu.VMEM((Z, OWN, HEADS * WIDE), F32),
+            pltpu.VMEM((4, OWN, HEADS * WIDE), BF16),
+            pltpu.VMEM((4, OWN, HEADS * WIDE), BF16),
+            pltpu.VMEM((4, OWN, HEADS * WIDE), BF16),
+            pltpu.VMEM((4, OWN, HEADS * WIDE), BF16),
             pltpu.VMEM((Z, HEADS, OWN, HEAD), BF16),
             pltpu.VMEM((Y, C, X, FEATS // X, SET), BF16),
-            pltpu.VMEM((X, G, FEATS // X, SET), BF16),
+            pltpu.VMEM((X * G, FEATS // X, SET), BF16),
             pltpu.SemaphoreType.REGULAR((3,)),
-            pltpu.SemaphoreType.DMA((21,)),
-            dma(G - 1),
-            dma(G - 1),
-            dma(Z - 1),
-            dma((HEADS + 1) * 7),
-            dma(HEADS * 4),
-            dma(HEADS * 4),
-            dma(HEADS * 7),
-            dma(G * X - 1),
+            pltpu.SemaphoreType.DMA((13,)),
+            pltpu.SemaphoreType.DMA((KINDS,)),
+            pltpu.SemaphoreType.DMA((ARRIVALS,)),
         ],
         compiler_params=pltpu.CompilerParams(collective_id=0, has_side_effects=True),
     )(*args)

time: 51.6 us -> 49.2 us (0.953)
  Pallas kernels: 50.9 us -> 48.4 us
    pallas_call x1, Pallas kernels: 48.9 us -> 46.4 us  [fused(): pl.pallas_call(kernel, out_shape=(pltpu.VMEM((G, FEATS // X, SET), BF16),...]
where the time goes in v4:
time: 49.2 us; the launch traced here: 49.1 us
  Pallas kernels  48.4 us (98%)
  between operations  0.64 us (1%)
    pallas_call x1, Pallas kernels, fused(): pl.pallas_call(kernel, out_shape=(pltpu.VMEM((G, FEATS // X, SET), BF16),...  46.4 us
    pallas_call x1, Pallas kernels, fused(): pl.pallas_call(tail, out_shape=(jax.ShapeDtypeStruct((FEATS // X, TOKENS)...  2.01 us

profile of v4, /device:TPU:1, one launch (start us, length us, event | category | flops | bytes accessed | tf_op | source)
XLA Modules:
  0.0 49.1 jit_solution(10543952034776535152)
XLA Ops:
  0.6 46.4 %shard_map.131 = (bf16[8,16,256]{2,1,0:T(8,128)(2,1)S(1)}, f32[8,4,128,128]{3,2,1,0:T(8,128)S(1)}) custom-call(bf16[64,2048]{1,0:T(8,128)(2,1)} %bitcast.6, bf16[1,64]{1,0:T(2,128)(2,1)} %bitcast.10, bf16[64,512]{1,0:T(8,128)(2,1)} %wq_hbm.1, bf16[64,512]{1,0:T(8,128)(2,1)} %wf_hbm.1, bf16[64,512]{1,0:T(8,128)(2,1)} %wv_hbm.1, bf16[64,512]{1,0:T(8,128)(2,1)} %bitcast.7, ...), custom_call_target="tpu_custom_call" | custom-call | tf_op jit(solution)/shard_map/pallas_call | solution.py:476
  47.1 2.0 %shard_map.132 = (bf16[16,2048]{1,0:T(8,128)(2,1)}, f32[8,4,128,128]{3,2,1,0:T(8,128)}) custom-call(bf16[8,16,256]{2,1,0:T(8,128)(2,1)S(1)} %get-tuple-element.6.pieces_ref, f32[8,4,128,128]{3,2,1,0:T(8,128)S(1)} %get-tuple-element.7.base_ref), custom_call_target="tpu_custom_call" | custom-call | tf_op jit(solution)/shard_map/pallas_call | solution.py:519

commit v5 on v4

--- a/solution.py
+++ b/solution.py
@@ -33,8 +33,8 @@
 HOPS = ((4, 3), (3, 4), (4, 3), (3, 4))
 SLOT = (0, 1, 3, 2)
 MERGES = {4: ((4, 3), (2, 1)), 3: ((3, 2), (None, 1))}
-KINDS = 10
-ARRIVALS = 36
+KINDS = 11
+ARRIVALS = 35
 
 
 def kernel(
@@ -189,10 +189,12 @@
         sem = recv_sems.at[arrivals[kind, arrival]]
         pltpu.make_async_copy(ref, ref, sem).wait()
 
-    for dy in (2, 1, 3):
+    quarter = FEATS // X
+    mine = pl.ds(pl.multiple_of(x * quarter, quarter), quarter)
+    for dy in (1, 3, 2):
         py = at_y(dy)
-        src = x_send.at[pl.ds(py * C, C)]
-        go(src, x_all.at[SLOT[dy]], "x", dy, (z, py, c, x))
+        src = x_send.at[pl.ds(py * C, C), mine]
+        go(src, x_all.at[SLOT[dy], :, mine], "x", 0, (z, py, c, x))
     x_all[0] = x_send[pl.ds(y * C, C)]
 
     for i, (dy, dc) in enumerate(group_steps):
@@ -203,7 +205,7 @@
         for copy in w_loads[j]:
             copy.wait()
         cols = pl.ds(start, width)
-        for dy in (2, 1, 3):
+        for dy in (1, 3, 2):
             dst = w_all.at[SLOT[dy], :, cols]
             go(w_all.at[0, :, cols], dst, "w", j, (z, at_y(dy), c, x))
     w_loads[-1][0].wait()
@@ -276,12 +278,19 @@
         )
         return lax.rsqrt(own_squares / D + EPSILON)
 
-    def inputs_in(pair):
-        for dy in ((1,), (3, 2))[pair]:
-            await_bytes(x_all.at[SLOT[dy]], "x", dy)
-        for k in range(C):
-            block = jnp.concatenate((x_all[2 * pair, k], x_all[2 * pair + 1, k]), axis=0)
-            left_ref[k, :, pl.ds(pair * HEAD, HEAD)] = jnp.transpose(block)
+    def inputs_across():
+        rows = x_all.at[pl.ds(1, Y - 1), :, mine]
+        await_bytes(rows, "x", 0)
+        for dx in (1, 3, 2):
+            go(rows, rows, "x across", 0, (z, y, c, at_x(dx)))
+
+    def inputs_in():
+        others = x_all.at[pl.ds(1, Y - 1), :, pl.ds(0, FEATS - quarter)]
+        await_bytes(others, "x across", 0)
+        for pair in range(Y // 2):
+            for k in range(C):
+                block = jnp.concatenate((x_all[2 * pair, k], x_all[2 * pair + 1, k]), axis=0)
+                left_ref[k, :, pl.ds(pair * HEAD, HEAD)] = jnp.transpose(block)
 
     def multiply(j):
         start, width = CHUNKS[j]
@@ -377,10 +386,10 @@
 
     relay_in(0)
     relay_out(1)
-    inputs_in(0)
+    inputs_across()
     relay_in(1)
     relay_out(2)
-    inputs_in(1)
+    inputs_in()
     multiply(0)
     distribute(0)
     multiply(1)
@@ -432,7 +441,8 @@
         out_ref[k] = total.astype(BF16)
 
     sent = {
-        "x": x_all.at[pl.ds(1, Y - 1)],
+        "x": x_all.at[pl.ds(1, Y - 1), :, pl.ds(0, quarter)],
+        "x across": x_all.at[pl.ds(1, Y - 1), :, pl.ds(0, FEATS - quarter)],
         "w": w_all.at[pl.ds(1, Y - 1)],
         "sq": sq_all,
         "wo": wo_all.at[pl.ds(0, G - 1)],

time: 49.2 us -> 48.3 us (0.982)
  Pallas kernels: 48.4 us -> 47.5 us
    pallas_call x1, Pallas kernels: 46.4 us -> 45.5 us  [fused(): pl.pallas_call(kernel, out_shape=(pltpu.VMEM((G, FEATS // X, SET), BF16),...]
where the time goes in v5:
time: 48.3 us; the launch traced here: 48.2 us
  Pallas kernels  47.5 us (98%)
  between operations  0.64 us (1%)
    pallas_call x1, Pallas kernels, fused(): pl.pallas_call(kernel, out_shape=(pltpu.VMEM((G, FEATS // X, SET), BF16),...  45.5 us
    pallas_call x1, Pallas kernels, fused(): pl.pallas_call(tail, out_shape=(jax.ShapeDtypeStruct((FEATS // X, TOKENS)...  2.01 us

profile of v5, /device:TPU:1, one launch (start us, length us, event | category | flops | bytes accessed | tf_op | source)
XLA Modules:
  0.0 48.2 jit_solution(18288956017357878925)
XLA Ops:
  0.6 45.5 %shard_map.131 = (bf16[8,16,256]{2,1,0:T(8,128)(2,1)S(1)}, f32[8,4,128,128]{3,2,1,0:T(8,128)S(1)}) custom-call(bf16[64,2048]{1,0:T(8,128)(2,1)} %bitcast.6, bf16[1,64]{1,0:T(2,128)(2,1)} %bitcast.10, bf16[64,512]{1,0:T(8,128)(2,1)} %wq_hbm.1, bf16[64,512]{1,0:T(8,128)(2,1)} %wf_hbm.1, bf16[64,512]{1,0:T(8,128)(2,1)} %wv_hbm.1, bf16[64,512]{1,0:T(8,128)(2,1)} %bitcast.7, ...), custom_call_target="tpu_custom_call" | custom-call | tf_op jit(solution)/shard_map/pallas_call | solution.py:486
  46.2 2.0 %shard_map.132 = (bf16[16,2048]{1,0:T(8,128)(2,1)}, f32[8,4,128,128]{3,2,1,0:T(8,128)}) custom-call(bf16[8,16,256]{2,1,0:T(8,128)(2,1)S(1)} %get-tuple-element.6.pieces_ref, f32[8,4,128,128]{3,2,1,0:T(8,128)S(1)} %get-tuple-element.7.base_ref), custom_call_target="tpu_custom_call" | custom-call | tf_op jit(solution)/shard_map/pallas_call | solution.py:529
